TPU v7x, 32 devices: a whole 2x2x4 slice. The times are simulated.
32 devices in a mesh: sp: 8 (over z, y), tp: 4 (over x, core).
Axes of the slice: x: 2, y: 2, z: 4, core: 2. Of those that a mesh axis runs over, the one named last changes fastest.
Arguments:
- residual: bfloat16 [3072, 2048], P(('sp', 'tp')), may hold values from -6 to 6
- query_one: bfloat16 [3072, 512], P('sp', 'tp'), may hold values from -6 to 6
- key_one: bfloat16 [3072, 512], P('sp', 'tp'), may hold values from -6 to 6
- value_one: bfloat16 [3072, 1024], P('sp', 'tp'), may hold values from -6 to 6
- gate_one: bfloat16 [3072, 1024], P('sp', 'tp'), may hold values from -6 to 6
- decay_one: bfloat16 [2, 3072, 512], P(None, 'sp', 'tp'), may hold values from -12 to 12
- norm_one: float32 [128], replicated, may hold values from 0.1 to 1.9
- output_one: bfloat16 [1024, 2048], P('tp'), may hold values from -0.125 to 0.125
- query_two: bfloat16 [3072, 1024], P('sp', 'tp'), may hold values from -6 to 6
- key_two: bfloat16 [3072, 1024], P('sp', 'tp'), may hold values from -6 to 6
- value_two: bfloat16 [3072, 1024], P('sp', 'tp'), may hold values from -6 to 6
- gate_two: bfloat16 [3072, 1024], P('sp', 'tp'), may hold values from -6 to 6
- decay_two: bfloat16 [2, 3072, 1024], P(None, 'sp', 'tp'), may hold values from -12 to 12
- norm_two: float32 [128], replicated, may hold values from 0.1 to 1.9
- output_two: bfloat16 [1024, 2048], P('tp'), may hold values from -0.125 to 0.125
- norm_gain: float32 [2048], replicated, may hold values from 0.1 to 1.9
- expert_ids: int32 [3072, 2], P('sp'), may hold values from 0 to 7, as said below
- group_weight: float32 [3072], P('sp'), may hold values from 0.25 to 1
- pair_weight: float32 [3072, 2], P('sp'), may hold values from 0.05 to 1
- expert_gate: bfloat16 [8, 2048, 1024], P('sp', None, 'tp'), may hold values from -0.125 to 0.125
- expert_up: bfloat16 [8, 2048, 1024], P('sp', None, 'tp'), may hold values from -0.125 to 0.125
- expert_down: bfloat16 [8, 1024, 2048], P('sp', 'tp'), may hold values from -0.1875 to 0.1875
Outputs:
- layer_out: bfloat16 [3072, 2048], P(('sp', 'tp'))
Inputs may be any that keep to these rules, and one draw needn't show every extreme that they name: `expert_ids`: each row names two different experts of one group, the group of expert e being e // 2. In each aligned block of 96 rows no expert is named more than 49 times, and one expert, the same in every block, is named exactly 49 times in each block.
All inputs are finite; a program needn't handle non-finite values.
Results may differ from a plain program's by a relative error of at most 0.018.
Values may be sent and summed in bfloat16 or wider, within the bound.
A program may use at most 128 MiB of HBM per device.

v0:
```python
import functools

import jax
import jax.numpy as jnp
from jax import lax
from jax.experimental import pallas as pl
from jax.experimental.pallas import tpu as pltpu
from jax.sharding import PartitionSpec as P

D = 2048
KEY_ONE = 64
KEY_TWO = 128
VALUE_W = 128
BLOCK = 64
GROUPS = 4


MESH = pl.DeviceIdType.MESH
TAU = 16.0
EPS = 1e-06


def log_sigmoid(x):
    return jnp.minimum(x, 0.0) - jnp.log1p(jnp.exp(-jnp.abs(x)))


def contract(a, b, dims):
    return lax.dot_general(a, b, (dims, ((), ())), preferred_element_type=jnp.float32)


NN, NT, TN = ((1,), (0,)), ((1,), (1,)), ((0,), (0,))


def flip_bit(index, bit):
    return index + bit - 2 * bit * lax.rem(index // bit, 2)


def meet(peers):
    barrier = pltpu.get_barrier_semaphore()
    for peer in peers:
        pl.semaphore_signal(barrier, inc=1, device_id=peer, device_id_type=MESH)
    pl.semaphore_wait(barrier, len(peers))


def mixer_kernel(
    n_sp,
    n_tp,
    q1,
    k1,
    v1,
    g1,
    d1,
    q2,
    k2,
    v2,
    g2,
    d2,
    norm1,
    norm2,
    out1,
    out2,
    res,
    gain,
    stream_ref,
    normed_ref,
    cum,
    qd,
    kd,
    added,
    ends,
    sent,
    got,
    carried,
    total,
    mixed,
    part_send,
    part_got,
    st_send,
    st_recv,
    pt_send,
    pt_recv,
):
    sp, tp = lax.axis_index("sp"), lax.axis_index("tp")
    length = q1.shape[0]
    blocks = length // BLOCK
    lanes = 128
    units = []
    for q, k, v, g, d, norm, key in (
        (q1, k1, v1, g1, d1, norm1, KEY_ONE),
        (q2, k2, v2, g2, d2, norm2, KEY_TWO),
    ):
        per = lanes // key
        for at in range(q.shape[1] // lanes):
            units.append((q, k, v, g, d, norm, key, per, at))
    count = len(units)
    bits = [1 << r for r in range(n_tp.bit_length() - 1)]

    meet(
        [(lax.rem(sp + off, n_sp), tp) for off in range(1, n_sp)]
        + [(sp, flip_bit(tp, bit)) for bit in bits]
    )

    t_at = lax.broadcasted_iota(jnp.int32, (length, length), 0)
    s_at = lax.broadcasted_iota(jnp.int32, (length, length), 1)
    same = (t_at // BLOCK) == (s_at // BLOCK)
    for way in range(2):
        tri = jnp.where(same & ((s_at <= t_at) if way == 0 else (s_at >= t_at)), 1.0, 0.0).astype(
            jnp.bfloat16
        )
        for u, (q, k, v, g, d, norm, key, per, at) in enumerate(units):
            cols = slice(at * lanes, (at + 1) * lanes)
            rate = log_sigmoid(d[way, :, cols].astype(jnp.float32)) / TAU
            high = rate.astype(jnp.bfloat16)
            rest = rate - high.astype(jnp.float32)
            mid = rest.astype(jnp.bfloat16)
            low = (rest - mid.astype(jnp.float32)).astype(jnp.bfloat16)
            cum[u] = contract(tri, high, NN) + contract(tri, mid, NN) + contract(tri, low, NN)
            state = jnp.zeros((VALUE_W, lanes), jnp.float32)
            reach = jnp.zeros((1, lanes), jnp.float32)
            lane = lax.broadcasted_iota(jnp.int32, (VALUE_W, lanes), 1) // key
            for n in range(blocks) if way == 0 else range(blocks - 1, -1, -1):
                rows = slice(n * BLOCK, (n + 1) * BLOCK)
                c = cum[u, rows, :]
                e = c[BLOCK - 1 : BLOCK] if way == 0 else c[0:1]
                queries = q[rows, cols].astype(jnp.float32) * key ** (-0.5)
                keys = k[rows, cols].astype(jnp.float32)
                qd[way, u, rows, :] = (queries * jnp.exp(c)).astype(jnp.bfloat16)
                kd[way, u, rows, :] = (keys * jnp.exp(-c)).astype(jnp.bfloat16)
                end = (keys * jnp.exp(e - c)).astype(jnp.bfloat16)
                term = None
                for h in range(per):
                    head = at * per + h
                    value = v[rows, head * VALUE_W : (head + 1) * VALUE_W]
                    new = contract(value, end, TN)
                    term = new if term is None else jnp.where(lane == h, new, term)
                added[way, u, n] = term
                fade = jnp.exp(e)
                ends[way, u, n : n + 1, :] = fade
                state = state * fade + term
                reach = reach + e
            sent[way, u * VALUE_W : (u + 1) * VALUE_W, :] = state.astype(jnp.bfloat16)
            sent[way, count * VALUE_W + 16 * u : count * VALUE_W + 16 * (u + 1), :] = (
                jnp.broadcast_to(jnp.exp(reach), (16, lanes)).astype(jnp.bfloat16)
            )

    def state_copy(off):
        to = lax.rem(sp + off, n_sp)
        way = jnp.where(to > sp, 0, 1)
        return pltpu.make_async_remote_copy(
            src_ref=sent.at[way],
            dst_ref=got.at[off],
            send_sem=st_send.at[off],
            recv_sem=st_recv.at[off],
            device_id=(to, tp),
            device_id_type=MESH,
        )

    @pl.loop(1, n_sp)
    def _(off):
        state_copy(off).start()

    t_blk = lax.broadcasted_iota(jnp.int32, (BLOCK, BLOCK), 0)
    s_blk = lax.broadcasted_iota(jnp.int32, (BLOCK, BLOCK), 1)
    first = 0
    for u, (q, k, v, g, d, norm, key, per, at) in enumerate(units):
        lane = lax.broadcasted_iota(jnp.int32, (BLOCK, lanes), 1) // key
        for h in range(per):
            head = at * per + h
            for n in range(blocks):
                rows = slice(n * BLOCK, (n + 1) * BLOCK)
                scores = None
                for way in range(2):
                    queries = qd[way, u, rows, :]
                    if per > 1:
                        queries = jnp.where(lane == h, queries, jnp.zeros_like(queries))
                    one = contract(queries, kd[way, u, rows, :], NT)
                    one = jnp.where((s_blk <= t_blk) if way == 0 else (s_blk >= t_blk), one, 0.0)
                    scores = one if scores is None else scores + one
                value = v[rows, head * VALUE_W : (head + 1) * VALUE_W]
                total[first + h, rows, :] = contract(scores.astype(jnp.bfloat16), value, NN)
        first += per

    @pl.loop(1, n_sp)
    def _(off):
        state_copy(off).wait()

    carried[...] = jnp.zeros_like(carried)

    def fold(way, who):
        off = lax.rem(sp - who + n_sp, n_sp)
        for u in range(count):
            fade = got[off, count * VALUE_W + 16 * u : count * VALUE_W + 16 * (u + 1), :][0:1]
            state = got[off, u * VALUE_W : (u + 1) * VALUE_W, :]
            carried[way, u] = carried[way, u] * fade.astype(jnp.float32) + state.astype(jnp.float32)

    @pl.loop(0, sp)
    def _(who):
        fold(0, who)

    @pl.loop(0, n_sp - 1 - sp)
    def _(back):
        fold(1, n_sp - 1 - back)

    first = 0
    for u, (q, k, v, g, d, norm, key, per, at) in enumerate(units):
        lane = lax.broadcasted_iota(jnp.int32, (BLOCK, lanes), 1) // key
        for way in range(2):
            state = carried[way, u]
            for n in range(blocks) if way == 0 else range(blocks - 1, -1, -1):
                rows = slice(n * BLOCK, (n + 1) * BLOCK)
                low = state.astype(jnp.bfloat16)
                for h in range(per):
                    queries = qd[way, u, rows, :]
                    if per > 1:
                        queries = jnp.where(lane == h, queries, jnp.zeros_like(queries))
                    total[first + h, rows, :] += contract(queries, low, NT)
                state = state * ends[way, u, n : n + 1, :] + added[way, u, n]
        for h in range(per):
            head = at * per + h
            cols = slice(head * VALUE_W, (head + 1) * VALUE_W)
            x = total[first + h]
            y = x * lax.rsqrt(jnp.mean(x * x, axis=-1, keepdims=True) + EPS) * norm[...]
            gate = g[:, cols].astype(jnp.float32)
            y = y * (gate / (1.0 + jnp.exp(-gate)))
            mixed[:, (first + h) * VALUE_W : (first + h + 1) * VALUE_W] = y.astype(jnp.bfloat16)
        first += per

    rows_dev = res.shape[0]
    split = out1.shape[0]

    def project(mask):
        block = tp
        for bit in bits:
            if mask & bit:
                block = flip_bit(block, bit)
        rows = pl.ds(pl.multiple_of(block * rows_dev, 16), rows_dev)
        return contract(mixed[rows, :split], out1[...], NN) + contract(
            mixed[rows, split:], out2[...], NN
        )

    def part_copy(mask, bit):
        return pltpu.make_async_remote_copy(
            src_ref=part_send.at[mask],
            dst_ref=part_got.at[mask],
            send_sem=pt_send.at[mask],
            recv_sem=pt_recv.at[mask],
            device_id=(sp, flip_bit(tp, bit)),
            device_id_type=MESH,
        )

    low_bit = lambda m: m & -m
    order = sorted(range(1, n_tp), key=lambda m: (low_bit(m), -m))
    for mask in order:
        bit = low_bit(mask)
        value = project(mask)
        for earlier in bits:
            if earlier < bit:
                part_copy(mask | earlier, earlier).wait_recv()
                value = value + part_got[mask | earlier].astype(jnp.float32)
        part_send[mask] = value.astype(jnp.bfloat16)
        part_copy(mask, bit).start()
    value = project(0)
    for bit in bits:
        part_copy(bit, bit).wait_recv()
        value = value + part_got[bit].astype(jnp.float32)
    stream = (res[...].astype(jnp.float32) + value.astype(jnp.bfloat16).astype(jnp.float32)).astype(
        jnp.bfloat16
    )
    stream_ref[...] = stream
    wide = stream.astype(jnp.float32)
    scale = lax.rsqrt(jnp.mean(wide * wide, axis=-1, keepdims=True) + EPS)
    normed_ref[...] = (wide * scale * gain[...]).astype(jnp.bfloat16)
    for mask in order:
        part_copy(mask, low_bit(mask)).wait_send()


def mixer(n_sp, n_tp, args, residual, norm_gain):
    q1, k1, v1, g1, d1, norm1, out1, q2, k2, v2, g2, d2, norm2, out2 = args
    length = q1.shape[0]
    blocks = length // BLOCK
    count = (q1.shape[1] + q2.shape[1]) // 128
    heads = (v1.shape[1] + v2.shape[1]) // VALUE_W
    rows, width = residual.shape
    packed = count * (VALUE_W + 16)
    bf, f32 = jnp.bfloat16, jnp.float32
    vmem = pl.BlockSpec(memory_space=pltpu.VMEM)
    sem = pltpu.SemaphoreType.DMA
    return pl.pallas_call(
        functools.partial(mixer_kernel, n_sp, n_tp),
        out_shape=(jax.ShapeDtypeStruct((rows, width), bf),) * 2,
        in_specs=[vmem] * 16,
        out_specs=(vmem, vmem),
        scratch_shapes=[
            pltpu.VMEM((count, length, 128), f32),
            pltpu.VMEM((2, count, length, 128), bf),
            pltpu.VMEM((2, count, length, 128), bf),
            pltpu.VMEM((2, count, blocks, VALUE_W, 128), f32),
            pltpu.VMEM((2, count, -(-blocks // 8) * 8, 128), f32),
            pltpu.VMEM((2, packed, 128), bf),
            pltpu.VMEM((n_sp, packed, 128), bf),
            pltpu.VMEM((2, count, VALUE_W, 128), f32),
            pltpu.VMEM((heads, length, VALUE_W), f32),
            pltpu.VMEM((length, heads * VALUE_W), bf),
            pltpu.VMEM((n_tp, rows, width), bf),
            pltpu.VMEM((n_tp, rows, width), bf),
            sem((n_sp,)),
            sem((n_sp,)),
            sem((n_tp,)),
            sem((n_tp,)),
        ],
        compiler_params=pltpu.CompilerParams(
            collective_id=0, has_side_effects=True, vmem_limit_bytes=60 * 2**20
        ),
    )(
        q1, k1, v1, g1, d1, q2, k2, v2, g2, d2,
        norm1[None], norm2[None], out1, out2, residual, norm_gain[None],
    )


def expert_kernel(
    stride, span, stream, normed, weight, slot, w_gate, w_up, w_down, out_ref,
    v_gate, v_up, v_down, z_send, z_got, data, part, from_core, from_x, from_y, back_got,
    w_sem, s_sem, r_sem,
):
    sp, tp = lax.axis_index("sp"), lax.axis_index("tp")
    width = normed.shape[1]
    half = (data.shape[1] // 32 + 1) * 16 if (data.shape[1] // 16) % 2 else data.shape[1] // 2
    top, low = slice(0, half), slice(half, data.shape[1])
    place, side = sp // 2, lax.rem(sp, 2)
    core, across, along = (sp, flip_bit(tp, 1)), (sp, flip_bit(tp, 2)), (flip_bit(sp, 1), tp)
    far = [(lax.rem(place + off, GROUPS), off) for off in range(1, GROUPS)]
    loads = [
        pltpu.make_async_copy(source, target, w_sem.at[i])
        for i, (source, target) in enumerate(((w_gate, v_gate), (w_up, v_up), (w_down, v_down)))
    ]
    for load in loads:
        load.start()
    meet([(z * 2 + side, tp) for z, _ in far] + [core, across, along])

    def copy(number, source, target, device):
        return pltpu.make_async_remote_copy(
            src_ref=source,
            dst_ref=target,
            send_sem=s_sem.at[number],
            recv_sem=r_sem.at[number],
            device_id=device,
            device_id_type=MESH,
        )

    rows = slot.shape[1]
    spread = (
        lax.broadcasted_iota(jnp.int32, (GROUPS * span, rows), 0) == slot[...]
    ).astype(jnp.float32).astype(jnp.bfloat16)
    high = weight[...].astype(jnp.bfloat16)
    rest = (weight[...] - high.astype(jnp.float32)).astype(jnp.bfloat16)
    z_send[:, :width] = contract(spread, normed[...], NN).astype(jnp.bfloat16)
    second = lax.broadcasted_iota(jnp.int32, high.shape, 1) >= 64
    both = jnp.where(second, rest.astype(jnp.float32), high.astype(jnp.float32))
    z_send[:, width:] = contract(spread, both.astype(jnp.bfloat16), NN).astype(jnp.bfloat16)

    def block(index):
        return pl.ds(pl.multiple_of(index * span, 16), span)

    def turn(index):
        return pl.ds(pl.multiple_of(index * stride, 16), span)

    outs = [copy(off, z_send.at[block(z)], z_got.at[off], (z * 2 + side, tp)) for z, off in far]
    for one in outs:
        one.start()
    data[0] = jnp.zeros(data.shape[1:], jnp.bfloat16)
    data[0, turn(place), :] = z_send[block(place), :]
    for one, (_, off) in zip(outs, far):
        one.wait()
        source = lax.rem(place - off + GROUPS, GROUPS)
        data[0, turn(source), :] = data[0, turn(source), :] + z_got[off]

    base = GROUPS
    c_0 = copy(base, data.at[0], data.at[1], core)
    a_y = copy(base + 1, data.at[0, top], data.at[2, top], along)
    b_x = copy(base + 2, data.at[0, low], data.at[4, low], across)
    a_x = copy(base + 3, data.at[0, top], data.at[4, top], across)
    b_y = copy(base + 4, data.at[0, low], data.at[2, low], along)
    a_d = copy(base + 5, data.at[2, top], data.at[6, top], across)
    b_d = copy(base + 6, data.at[4, low], data.at[6, low], along)
    c_y = copy(base + 7, data.at[2], data.at[3], core)
    c_x = copy(base + 8, data.at[4], data.at[5], core)
    c_d = copy(base + 9, data.at[6], data.at[7], core)
    base += 10
    p_c = [copy(base + i, part.at[2 * i + 1], from_core.at[i], core) for i in range(4)]
    base += 4
    r_ax = copy(base, part.at[4, top], from_x.at[0, top], across)
    r_by = copy(base + 1, part.at[2, low], from_y.at[0, low], along)
    r_ad = copy(base + 2, part.at[6, top], from_x.at[1, top], across)
    r_bd = copy(base + 3, part.at[6, low], from_y.at[1, low], along)
    r_ay = copy(base + 4, part.at[2, top], from_y.at[0, top], along)
    r_bx = copy(base + 5, part.at[4, low], from_x.at[0, low], across)
    base += 6
    for one in (a_y, b_x, a_x, b_y, c_0):
        one.start()

    for load in loads:
        load.wait()

    def compute(first, count):
        @pl.loop(first, first + count)
        def _(m):
            x = data[m, :, :width]
            w = data[m, :, width:].astype(jnp.float32)
            lane = lax.broadcasted_iota(jnp.int32, w.shape, 1)
            w = jnp.sum(jnp.where((lane == side) | (lane == side + 64), w, 0.0), axis=1, keepdims=True)
            gate = contract(x, v_gate[...], NN)
            up = contract(x, v_up[...], NN)
            hidden = (gate / (1.0 + jnp.exp(-gate)) * up * w).astype(jnp.bfloat16)
            part[m] = contract(hidden, v_down[...], NN).astype(jnp.bfloat16)

    def add(m, where, term):
        part[m, where, :] = (
            part[m, where, :].astype(jnp.float32) + term.astype(jnp.float32)
        ).astype(jnp.bfloat16)

    everything = slice(0, data.shape[1])
    c_0.wait_recv()
    compute(0, 2)
    p_c[0].start()
    a_y.wait_recv()
    a_d.start()
    b_x.wait_recv()
    b_d.start()
    b_y.wait_recv()
    c_y.start()
    a_x.wait_recv()
    c_x.start()
    c_y.wait_recv()
    c_x.wait_recv()
    compute(2, 4)
    p_c[1].start()
    p_c[2].start()
    p_c[1].wait_recv()
    add(2, everything, from_core[1])
    r_by.start()
    p_c[2].wait_recv()
    add(4, everything, from_core[2])
    r_ax.start()
    a_d.wait_recv()
    b_d.wait_recv()
    c_d.start()
    compute(6, 1)
    c_d.wait_recv()
    compute(7, 1)
    p_c[3].start()
    p_c[3].wait_recv()
    add(6, everything, from_core[3])
    r_ad.start()
    r_bd.start()
    p_c[0].wait_recv()
    r_ad.wait_recv()
    add(2, top, from_x[1, top])
    r_ay.start()
    r_bd.wait_recv()
    add(4, low, from_y[1, low])
    r_bx.start()
    r_ax.wait_recv()
    r_by.wait_recv()
    r_ay.wait_recv()
    r_bx.wait_recv()
    f32 = jnp.float32
    summed = part[0].astype(f32) + from_core[0].astype(f32)
    part[0] = (summed + from_x[0].astype(f32) + from_y[0].astype(f32)).astype(jnp.bfloat16)

    outs = []
    for z, off in far:
        outs.append(copy(base + off, part.at[0, turn(z)], back_got.at[block(place)], (z * 2 + side, tp)))
        outs[-1].start()
    back_got[block(place), :] = part[0, turn(place), :]
    for one in outs:
        one.wait_recv()
    picked = contract(spread, back_got[...], TN)
    out_ref[...] = (stream[...].astype(f32) + picked).astype(jnp.bfloat16)
    for one in [c_0, a_y, b_x, a_x, b_y, a_d, b_d, c_y, c_x, c_d] + p_c + outs:
        one.wait_send()
    for one in (r_ax, r_by, r_ad, r_bd, r_ay, r_bx):
        one.wait_send()


def grouped_experts(stream, normed, routes, weights, capacity, w_gate, w_up, w_down):
    rows, width = stream.shape
    stride = (capacity - 1) // 16 * 16
    if stride + 1 < capacity:
        stride += 16
    span = -(-(capacity + (GROUPS - 1) * max(0, capacity - stride)) // 16) * 16
    length = stride * (GROUPS - 1) + span
    group = routes[:, 0] // 2
    position = jnp.arange(rows, dtype=jnp.int32)
    ahead = (group[:, None] == group[None, :]) & (position[None, :] < position[:, None])
    nth = jnp.sum(ahead.astype(jnp.int32), axis=1)
    shift = lax.axis_index("sp") // 2 * max(0, capacity - stride)
    slot = (group * span + shift + nth)[None, :]
    side = routes[:, :, None] % 2 == (jnp.arange(128, dtype=jnp.int32) % 64)[None, None, :]
    weight = jnp.sum(jnp.where(side, weights[:, :, None], 0.0), axis=1)
    bf = jnp.bfloat16
    vmem = pl.BlockSpec(memory_space=pltpu.VMEM)
    hbm = pl.BlockSpec(memory_space=pl.ANY)
    sem = pltpu.SemaphoreType.DMA
    wide = width + 128
    copies = 2 * GROUPS + 20
    return pl.pallas_call(
        functools.partial(expert_kernel, stride, span),
        out_shape=jax.ShapeDtypeStruct((rows, width), bf),
        in_specs=[vmem] * 4 + [hbm] * 3,
        out_specs=vmem,
        scratch_shapes=[
            pltpu.VMEM(w_gate.shape, bf),
            pltpu.VMEM(w_up.shape, bf),
            pltpu.VMEM(w_down.shape, bf),
            pltpu.VMEM((GROUPS * span, wide), bf),
            pltpu.VMEM((GROUPS, span, wide), bf),
            pltpu.VMEM((8, length, wide), bf),
            pltpu.VMEM((8, length, width), bf),
            pltpu.VMEM((4, length, width), bf),
            pltpu.VMEM((2, length, width), bf),
            pltpu.VMEM((2, length, width), bf),
            pltpu.VMEM((GROUPS * span, width), bf),
            sem((3,)),
            sem((copies,)),
            sem((copies,)),
        ],
        compiler_params=pltpu.CompilerParams(
            collective_id=1, has_side_effects=True, vmem_limit_bytes=60 * 2**20
        ),
    )(stream, normed, weight, slot, w_gate, w_up, w_down)


def slot_table(routes, capacity, experts):
    flat = routes.reshape(-1)
    count = flat.shape[0]
    onehot = (flat[:, None] == jnp.arange(experts, dtype=jnp.int32)[None, :]).astype(jnp.int32)
    place = jnp.sum((jnp.cumsum(onehot, axis=0) - onehot) * onehot, axis=1)
    table = (
        jnp.full((experts, capacity), count, jnp.int32)
        .at[flat, place]
        .set(jnp.arange(count, dtype=jnp.int32))
    )
    return (table, place)


def body(
    residual,
    query_one,
    key_one,
    value_one,
    gate_one,
    decay_one,
    norm_one,
    output_one,
    query_two,
    key_two,
    value_two,
    gate_two,
    decay_two,
    norm_two,
    output_two,
    norm_gain,
    expert_ids,
    group_weight,
    pair_weight,
    expert_gate,
    expert_up,
    expert_down,
):
    stream, normed_rows = mixer(
        lax.axis_size("sp"),
        lax.axis_size("tp"),
        (
            query_one, key_one, value_one, gate_one, decay_one, norm_one, output_one,
            query_two, key_two, value_two, gate_two, decay_two, norm_two, output_two,
        ),
        residual,
        norm_gain,
    )
    rows_dev = residual.shape[0]
    rank = lax.axis_index("tp")
    experts = lax.axis_size("sp")
    capacity = max(2, 2 * rows_dev // (experts - GROUPS) + 1)
    own_routes = lax.dynamic_slice_in_dim(expert_ids, rank * rows_dev, rows_dev, 0)
    own_group = lax.dynamic_slice_in_dim(group_weight, rank * rows_dev, rows_dev, 0)
    own_pair = lax.dynamic_slice_in_dim(pair_weight, rank * rows_dev, rows_dev, 0)
    weights = own_group[:, None] * own_pair / jnp.sum(own_pair, axis=1, keepdims=True)
    if experts == 2 * GROUPS and lax.axis_size("tp") == 4:
        return grouped_experts(
            stream,
            normed_rows,
            own_routes,
            weights,
            capacity,
            expert_gate[0],
            expert_up[0],
            expert_down[0],
        )
    blank = jnp.zeros((1, D), jnp.bfloat16)
    table, own_place = slot_table(own_routes, capacity, experts)
    index = jnp.where(table == 2 * rows_dev, rows_dev, table // 2)
    send = jnp.concatenate([normed_rows, blank], axis=0)[index][None]
    received = lax.all_to_all(send, "sp", split_axis=1, concat_axis=1, tiled=True)
    received = lax.all_gather(received, "tp", axis=0, tiled=True)
    flat = received.reshape(-1, received.shape[-1])
    gate_part = jnp.dot(flat, expert_gate[0], preferred_element_type=jnp.float32)
    up_part = jnp.dot(flat, expert_up[0], preferred_element_type=jnp.float32)
    hidden = (jax.nn.silu(gate_part) * up_part).astype(jnp.bfloat16)
    share_sum = lax.psum_scatter(
        jnp.dot(hidden, expert_down[0], preferred_element_type=jnp.float32)
        .reshape(received.shape)
        .astype(jnp.bfloat16),
        "tp",
        scatter_dimension=0,
        tiled=True,
    )
    returned = lax.all_to_all(share_sum, "sp", split_axis=1, concat_axis=1, tiled=True)
    slot_index = own_routes.reshape(-1) * capacity + own_place
    picked = returned.reshape(-1, D)[slot_index].astype(jnp.float32).reshape(rows_dev, 2, D)
    layer = stream.astype(jnp.float32) + jnp.sum(weights[:, :, None] * picked, axis=1)
    return layer.astype(jnp.bfloat16)


def solution(mesh):
    placed = (
        P(("sp", "tp"), None),
        P("sp", "tp"),
        P("sp", "tp"),
        P("sp", "tp"),
        P("sp", "tp"),
        P(None, "sp", "tp"),
        P(),
        P("tp", None),
        P("sp", "tp"),
        P("sp", "tp"),
        P("sp", "tp"),
        P("sp", "tp"),
        P(None, "sp", "tp"),
        P(),
        P("tp", None),
        P(),
        P("sp", None),
        P("sp"),
        P("sp", None),
        P("sp", None, "tp"),
        P("sp", None, "tp"),
        P("sp", "tp", None),
    )
    return jax.shard_map(
        body, mesh=mesh, in_specs=placed, out_specs=P(("sp", "tp"), None), check_vma=False
    )
```

profile of v0, /device:TPU:0, one launch (start us, length us, event | category | flops | bytes accessed | tf_op | source)
XLA Modules:
  0.0 161.0 jit_solution(659832214187288711)
XLA Ops:
  0.0 0.0 copy-start
  0.0 0.8 dynamic_slice.10
  0.8 0.0 copy-done
  0.8 0.1 dynamic-slice_reduce_fusion
  0.9 0.1 multiply_divide_fusion
  0.9 0.8 and_select_fusion.4
  1.7 0.2 convert_reduce_fusion
  1.9 0.6 bitcast_add_fusion.slot
  2.5 0.7 select_reduce_fusion.weight
  3.2 42.2 %shard_map.208 = (bf16[96,2048]{1,0:T(8,128)(2,1)}, bf16[96,2048]{1,0:T(8,128)(2,1)}) custom-call(bf16[384,128]{1,0:T(8,128)(2,1)} %q1.1, bf16[384,128]{1,0:T(8,128)(2,1)} %k1.1, bf16[384,256]{1,0:T(8,128)(2,1)} %v1.1, bf16[384,256]{1,0:T(8,128)(2,1)} %g1.1, bf16[2,384,128]{2,1,0:T(8,128)(2,1)} %d1.1, bf16[384,256]{1,0:T(8,128)(2,1)} %q2.1, ...), custom_call_target="tpu_custom_call" | custom-call | tf_op jit(solution)/shard_map/pallas_call | solution.py:288
  45.4 113.7 %shard_map.209 = bf16[96,2048]{1,0:T(8,128)(2,1)} custom-call(bf16[96,2048]{1,0:T(8,128)(2,1)} %get-tuple-element.7.stream, bf16[96,2048]{1,0:T(8,128)(2,1)} %get-tuple-element.8.normed, f32[96,128]{1,0:T(8,128)} %select_reduce_fusion.weight, s32[1,96]{1,0:T(1,128)} %bitcast_add_fusion.slot, bf16[2048,256]{1,0:T(8,128)(2,1)} %bitcast.28, ...), custom_call_target="tpu_custom_call" | custom-call | tf_op jit(solution)/shard_map/pallas_call | solution.py:506
  159.2 1.8 %copy.26 = bf16[96,2048]{1,0:T(8,128)(2,1)} copy(bf16[96,2048]{1,0:T(8,128)(2,1)} %shard_map.209) | data formatting | bytes 786432
  (3 shorter events, 0.0 us)
Async XLA Ops:
  0.0 0.8 copy-start
where the time goes:
time: 164 us; the launch traced here: 161 us
  Pallas kernels  156 us (95%)
  local copies, waits for them, and re-layouts  2.54 us (2%)
  other arithmetic  2.46 us (2%)
    pallas_call x1, Pallas kernels, grouped_experts(): pl.pallas_call(functools.partial(expert_kernel, stride, span), out_shape=...  114 us
    pallas_call x1, Pallas kernels, mixer(): pl.pallas_call(functools.partial(mixer_kernel, n_sp, n_tp), out_shape=(ja...  42.2 us

commit v1 on v0

v1 whole, which is shorter than its diff:
```python
import functools

import jax
import jax.numpy as jnp
from jax import lax
from jax.experimental import pallas as pl
from jax.experimental.pallas import tpu as pltpu
from jax.sharding import PartitionSpec as P

D = 2048
KEY_ONE = 64
KEY_TWO = 128
VALUE_W = 128
BLOCK = 64
GROUPS = 4


MESH = pl.DeviceIdType.MESH
TAU = 16.0
EPS = 1e-06


def log_sigmoid(x):
    return jnp.minimum(x, 0.0) - jnp.log1p(jnp.exp(-jnp.abs(x)))


def contract(a, b, dims):
    return lax.dot_general(a, b, (dims, ((), ())), preferred_element_type=jnp.float32)


NN, NT, TN = ((1,), (0,)), ((1,), (1,)), ((0,), (0,))


def flip_bit(index, bit):
    return index + bit - 2 * bit * lax.rem(index // bit, 2)


def meet(peers):
    barrier = pltpu.get_barrier_semaphore()
    for peer in peers:
        pl.semaphore_signal(barrier, inc=1, device_id=peer, device_id_type=MESH)
    pl.semaphore_wait(barrier, len(peers))


def remote(source, target, send, recv, device):
    return pltpu.make_async_remote_copy(
        src_ref=source,
        dst_ref=target,
        send_sem=send,
        recv_sem=recv,
        device_id=device,
        device_id_type=MESH,
    )


def nothing(*_):
    return None


PACK = VALUE_W + 16


def mix(n_sp, n_tp, operands, scratch, ready, sent_states, got_states):
    q1, k1, v1, g1, d1, q2, k2, v2, g2, d2, norm1, norm2, out1, out2, res, gain = operands
    cum, qd, kd, added, ends, sent, got, carried, total, mixed, part_send, part_got = scratch[:12]
    st_send, st_recv, pt_send, pt_recv = scratch[12:]
    sp, tp = lax.axis_index("sp"), lax.axis_index("tp")
    length = q1.shape[0]
    blocks = length // BLOCK
    lanes = 128
    units = []
    for q, k, v, g, d, norm, key in (
        (q1, k1, v1, g1, d1, norm1, KEY_ONE),
        (q2, k2, v2, g2, d2, norm2, KEY_TWO),
    ):
        per = lanes // key
        for at in range(q.shape[1] // lanes):
            units.append((q, k, v, g, d, norm, key, per, at))
    count = len(units)
    bits = [1 << r for r in range(n_tp.bit_length() - 1)]

    meet(
        [(lax.rem(sp + off, n_sp), tp) for off in range(1, n_sp)]
        + [(sp, flip_bit(tp, bit)) for bit in bits]
        + ready(None)
    )
    ready(True)

    def state_copy(u, off):
        to = lax.rem(sp + off, n_sp)
        way = jnp.where(to > sp, 0, 1)
        rows = slice(u * PACK, (u + 1) * PACK)
        sem = off * count + u
        return remote(
            sent.at[way, rows], got.at[off, rows], st_send.at[sem], st_recv.at[sem], (to, tp)
        )

    t_at = lax.broadcasted_iota(jnp.int32, (length, length), 0)
    s_at = lax.broadcasted_iota(jnp.int32, (length, length), 1)
    same = (t_at // BLOCK) == (s_at // BLOCK)
    for u, (q, k, v, g, d, norm, key, per, at) in enumerate(units):
        for way in range(2):
            tri = jnp.where(
                same & ((s_at <= t_at) if way == 0 else (s_at >= t_at)), 1.0, 0.0
            ).astype(jnp.bfloat16)
            cols = slice(at * lanes, (at + 1) * lanes)
            rate = log_sigmoid(d[way, :, cols].astype(jnp.float32)) / TAU
            high = rate.astype(jnp.bfloat16)
            rest = rate - high.astype(jnp.float32)
            mid = rest.astype(jnp.bfloat16)
            low = (rest - mid.astype(jnp.float32)).astype(jnp.bfloat16)
            cum[u] = contract(tri, high, NN) + contract(tri, mid, NN) + contract(tri, low, NN)
            state = jnp.zeros((VALUE_W, lanes), jnp.float32)
            reach = jnp.zeros((1, lanes), jnp.float32)
            lane = lax.broadcasted_iota(jnp.int32, (VALUE_W, lanes), 1) // key
            for n in range(blocks) if way == 0 else range(blocks - 1, -1, -1):
                rows = slice(n * BLOCK, (n + 1) * BLOCK)
                c = cum[u, rows, :]
                e = c[BLOCK - 1 : BLOCK] if way == 0 else c[0:1]
                queries = q[rows, cols].astype(jnp.float32) * key ** (-0.5)
                keys = k[rows, cols].astype(jnp.float32)
                qd[way, u, rows, :] = (queries * jnp.exp(c)).astype(jnp.bfloat16)
                kd[way, u, rows, :] = (keys * jnp.exp(-c)).astype(jnp.bfloat16)
                end = (keys * jnp.exp(e - c)).astype(jnp.bfloat16)
                term = None
                for h in range(per):
                    head = at * per + h
                    value = v[rows, head * VALUE_W : (head + 1) * VALUE_W]
                    new = contract(value, end, TN)
                    term = new if term is None else jnp.where(lane == h, new, term)
                added[way, u, n] = term
                fade = jnp.exp(e)
                ends[way, u, n : n + 1, :] = fade
                state = state * fade + term
                reach = reach + e
            sent[way, u * PACK : u * PACK + VALUE_W, :] = state.astype(jnp.bfloat16)
            sent[way, u * PACK + VALUE_W : (u + 1) * PACK, :] = jnp.broadcast_to(
                jnp.exp(reach), (16, lanes)
            ).astype(jnp.bfloat16)

        @pl.loop(1, n_sp)
        def _(off):
            state_copy(u, off).start()

    sent_states()
    t_blk = lax.broadcasted_iota(jnp.int32, (BLOCK, BLOCK), 0)
    s_blk = lax.broadcasted_iota(jnp.int32, (BLOCK, BLOCK), 1)
    first = 0
    for u, (q, k, v, g, d, norm, key, per, at) in enumerate(units):
        lane = lax.broadcasted_iota(jnp.int32, (BLOCK, lanes), 1) // key
        for h in range(per):
            head = at * per + h
            for n in range(blocks):
                rows = slice(n * BLOCK, (n + 1) * BLOCK)
                scores = None
                for way in range(2):
                    queries = qd[way, u, rows, :]
                    if per > 1:
                        queries = jnp.where(lane == h, queries, jnp.zeros_like(queries))
                    one = contract(queries, kd[way, u, rows, :], NT)
                    one = jnp.where((s_blk <= t_blk) if way == 0 else (s_blk >= t_blk), one, 0.0)
                    scores = one if scores is None else scores + one
                value = v[rows, head * VALUE_W : (head + 1) * VALUE_W]
                total[first + h, rows, :] = contract(scores.astype(jnp.bfloat16), value, NN)
        first += per

    @pl.loop(1, n_sp)
    def _(off):
        for u in range(count):
            state_copy(u, off).wait()

    got_states()
    carried[...] = jnp.zeros_like(carried)

    def fold(way, who):
        off = lax.rem(sp - who + n_sp, n_sp)
        for u in range(count):
            fade = got[off, u * PACK + VALUE_W : (u + 1) * PACK, :][0:1]
            state = got[off, u * PACK : u * PACK + VALUE_W, :]
            carried[way, u] = carried[way, u] * fade.astype(jnp.float32) + state.astype(jnp.float32)

    @pl.loop(0, sp)
    def _(who):
        fold(0, who)

    @pl.loop(0, n_sp - 1 - sp)
    def _(back):
        fold(1, n_sp - 1 - back)

    first = 0
    for u, (q, k, v, g, d, norm, key, per, at) in enumerate(units):
        lane = lax.broadcasted_iota(jnp.int32, (BLOCK, lanes), 1) // key
        for way in range(2):
            state = carried[way, u]
            for n in range(blocks) if way == 0 else range(blocks - 1, -1, -1):
                rows = slice(n * BLOCK, (n + 1) * BLOCK)
                low = state.astype(jnp.bfloat16)
                for h in range(per):
                    queries = qd[way, u, rows, :]
                    if per > 1:
                        queries = jnp.where(lane == h, queries, jnp.zeros_like(queries))
                    total[first + h, rows, :] += contract(queries, low, NT)
                state = state * ends[way, u, n : n + 1, :] + added[way, u, n]
        for h in range(per):
            head = at * per + h
            cols = slice(head * VALUE_W, (head + 1) * VALUE_W)
            x = total[first + h]
            y = x * lax.rsqrt(jnp.mean(x * x, axis=-1, keepdims=True) + EPS) * norm[...]
            gate = g[:, cols].astype(jnp.float32)
            y = y * (gate / (1.0 + jnp.exp(-gate)))
            mixed[:, (first + h) * VALUE_W : (first + h + 1) * VALUE_W] = y.astype(jnp.bfloat16)
        first += per

    rows_dev = res.shape[0]
    split = out1.shape[0]

    def project(mask):
        block = tp
        for bit in bits:
            if mask & bit:
                block = flip_bit(block, bit)
        rows = pl.ds(pl.multiple_of(block * rows_dev, 16), rows_dev)
        return contract(mixed[rows, :split], out1[...], NN) + contract(
            mixed[rows, split:], out2[...], NN
        )

    def part_copy(mask, bit):
        return remote(
            part_send.at[mask],
            part_got.at[mask],
            pt_send.at[mask],
            pt_recv.at[mask],
            (sp, flip_bit(tp, bit)),
        )

    low_bit = lambda m: m & -m
    order = sorted(range(1, n_tp), key=lambda m: (low_bit(m), -m))
    for mask in order:
        bit = low_bit(mask)
        value = project(mask)
        for earlier in bits:
            if earlier < bit:
                part_copy(mask | earlier, earlier).wait_recv()
                value = value + part_got[mask | earlier].astype(jnp.float32)
        part_send[mask] = value.astype(jnp.bfloat16)
        part_copy(mask, bit).start()
    value = project(0)
    for bit in bits:
        part_copy(bit, bit).wait_recv()
        value = value + part_got[bit].astype(jnp.float32)
    stream = (res[...].astype(jnp.float32) + value.astype(jnp.bfloat16).astype(jnp.float32)).astype(
        jnp.bfloat16
    )
    wide = stream.astype(jnp.float32)
    scale = lax.rsqrt(jnp.mean(wide * wide, axis=-1, keepdims=True) + EPS)
    normed = (wide * scale * gain[...]).astype(jnp.bfloat16)
    return stream, normed, [part_copy(mask, low_bit(mask)) for mask in order]


def mix_scratch(n_sp, n_tp, args, residual):
    q1, k1, v1, g1, d1, norm1, out1, q2, k2, v2, g2, d2, norm2, out2 = args
    length = q1.shape[0]
    blocks = length // BLOCK
    count = (q1.shape[1] + q2.shape[1]) // 128
    heads = (v1.shape[1] + v2.shape[1]) // VALUE_W
    rows, width = residual.shape
    packed = count * PACK
    bf, f32 = jnp.bfloat16, jnp.float32
    sem = pltpu.SemaphoreType.DMA
    return [
        pltpu.VMEM((count, length, 128), f32),
        pltpu.VMEM((2, count, length, 128), bf),
        pltpu.VMEM((2, count, length, 128), bf),
        pltpu.VMEM((2, count, blocks, VALUE_W, 128), f32),
        pltpu.VMEM((2, count, -(-blocks // 8) * 8, 128), f32),
        pltpu.VMEM((2, packed, 128), bf),
        pltpu.VMEM((n_sp, packed, 128), bf),
        pltpu.VMEM((2, count, VALUE_W, 128), f32),
        pltpu.VMEM((heads, length, VALUE_W), f32),
        pltpu.VMEM((length, heads * VALUE_W), bf),
        pltpu.VMEM((n_tp, rows, width), bf),
        pltpu.VMEM((n_tp, rows, width), bf),
        sem((n_sp * count,)),
        sem((n_sp * count,)),
        sem((n_tp,)),
        sem((n_tp,)),
    ]


def mix_operands(args, residual, norm_gain):
    q1, k1, v1, g1, d1, norm1, out1, q2, k2, v2, g2, d2, norm2, out2 = args
    return (
        q1, k1, v1, g1, d1, q2, k2, v2, g2, d2,
        norm1[None], norm2[None], out1, out2, residual, norm_gain[None],
    )


def mixer_kernel(n_sp, n_tp, *refs):
    operands, (stream_ref, normed_ref), scratch = refs[:16], refs[16:18], refs[18:]
    ready = lambda go: [] if go is None else None
    stream, normed, pending = mix(n_sp, n_tp, operands, scratch, ready, nothing, nothing)
    stream_ref[...] = stream
    normed_ref[...] = normed
    for one in pending:
        one.wait_send()


def mixer(n_sp, n_tp, args, residual, norm_gain):
    rows, width = residual.shape
    vmem = pl.BlockSpec(memory_space=pltpu.VMEM)
    return pl.pallas_call(
        functools.partial(mixer_kernel, n_sp, n_tp),
        out_shape=(jax.ShapeDtypeStruct((rows, width), jnp.bfloat16),) * 2,
        in_specs=[vmem] * 16,
        out_specs=(vmem, vmem),
        scratch_shapes=mix_scratch(n_sp, n_tp, args, residual),
        compiler_params=pltpu.CompilerParams(
            collective_id=0, has_side_effects=True, vmem_limit_bytes=60 * 2**20
        ),
    )(*mix_operands(args, residual, norm_gain))


def nearest(place, rank):
    half, last = GROUPS // 2, GROUPS - 1
    turned = place // half
    inner = place + turned * (last - 2 * place)
    spot = rank + turned * 0
    if isinstance(rank, int):
        spot = rank + inner * (1 - 2 * rank) if rank < half else rank + 0 * inner
    return spot + turned * (last - 2 * spot)


def rank_of(place, other):
    half, last = GROUPS // 2, GROUPS - 1
    turned = place // half
    inner = place + turned * (last - 2 * place)
    spot = other + turned * (last - 2 * other)
    return spot + inner * (1 - spot // half) * (1 - 2 * spot)


KINDS = 5
COPIES = 10 * GROUPS + 4 * GROUPS + 8


def layer_kernel(n_sp, n_tp, stride, extra, n_scratch, *refs):
    operands = refs[:16]
    weight, slot, w_gate, w_up, w_down, out_ref = refs[16:22]
    scratch = refs[22 : 22 + n_scratch]
    (
        v_gate, v_up, wd, spread, meta_send, meta_got, wslot, z_send, z_extra, data, hid, hgot,
        acc, part, pgot, outs, back_got, kept, w_sem, s_sem, r_sem, zs_sem, zr_sem,
    ) = refs[22 + n_scratch :]
    bf, f32 = jnp.bfloat16, jnp.float32
    sp, tp = lax.axis_index("sp"), lax.axis_index("tp")
    span = stride + extra
    length = GROUPS * stride + extra
    width = data.shape[2]
    units = hid.shape[2]
    place, side = sp // 2, lax.rem(sp, 2)
    core, across, along = (sp, flip_bit(tp, 1)), (sp, flip_bit(tp, 2)), (flip_bit(sp, 1), tp)
    corner = (flip_bit(sp, 1), flip_bit(tp, 2))
    left, right = slice(0, width // 2), slice(width // 2, width)
    far = []
    for i in range(1, GROUPS):
        z = nearest(place, i)
        far.append((i, rank_of(z, place), (z * 2 + side, tp)))
    numbers = iter(range(COPIES))
    started = []

    def copy(source, target, device):
        number = next(numbers)
        return remote(source, target, s_sem.at[number], r_sem.at[number], device)

    def go(one):
        one.start()
        started.append(one)
        return one

    def z_copy(kind, i, rank, source, target, device):
        return remote(
            source,
            target,
            zs_sem.at[kind * GROUPS + i],
            zr_sem.at[kind * GROUPS + rank],
            device,
        )

    loads = [
        pltpu.make_async_copy(source, target, w_sem.at[i])
        for i, (source, target) in enumerate(
            ((w_gate, v_gate), (w_up, v_up), (w_down, wd.at[0]))
        )
    ]
    early = units // 4
    down_y = [
        copy(w_down.at[rows], wd.at[1, rows], along)
        for rows in (slice(0, early), slice(early, units))
    ]
    down_x = copy(w_down, wd.at[2], across)
    upper, lower = slice(0, units // 2), slice(units // 2, units)
    down_yx = copy(wd.at[1, upper], wd.at[3, upper], across)
    down_xy = copy(wd.at[2, lower], wd.at[3, lower], along)
    metas = [
        z_copy(4, i, rank, meta_send.at[slice(i * span, (i + 1) * span)], meta_got.at[rank], to)
        for i, rank, to in far
    ]
    meta_core = copy(wslot.at[0], wslot.at[1], core)

    def block(index):
        return slice(index * span, (index + 1) * span)

    def chunk(o):
        return slice(o * stride, (o + 1) * stride if o < GROUPS - 1 else length)

    def ready(begin):
        if begin is None:
            return [core_peer for core_peer in (corner,)]
        for load in loads:
            load.start()
        go(down_x)
        go(down_y[0])
        rows = slot.shape[1]
        spread[...] = (
            (lax.broadcasted_iota(jnp.int32, (GROUPS * span, rows), 0) == slot[...])
            .astype(f32)
            .astype(bf)
        )
        high = weight[...].astype(bf)
        rest = (weight[...] - high.astype(f32)).astype(bf)
        second = lax.broadcasted_iota(jnp.int32, high.shape, 1) >= 64
        both = jnp.where(second, rest.astype(f32), high.astype(f32)).astype(bf)
        meta_send[...] = contract(spread[...], both, NN).astype(bf)
        for one in metas:
            go(one)

    def sent_states():
        go(down_y[1])

    def meta_wait(o):
        z_copy(4, 0, o, meta_send.at[block(o)], meta_got.at[o], core).wait_recv()

    def got_states():
        own = meta_send[block(0)]
        wslot[0, 0:stride] = own[:stride]
        more = own[stride:].astype(f32)
        for o in range(1, GROUPS):
            meta_wait(o)
            wslot[0, o * stride : (o + 1) * stride] = meta_got[o, :stride]
            more = more + meta_got[o, stride:].astype(f32)
        wslot[0, GROUPS * stride :] = more.astype(bf)
        go(meta_core)

    stream, normed, pending = mix(n_sp, n_tp, operands, scratch, ready, sent_states, got_states)
    kept[...] = stream

    for i, rank, to in far:
        z_send[block(i)] = contract(spread[block(i), :], normed, NN).astype(bf)
        go(
            z_copy(
                0, i, rank,
                z_send.at[slice(i * span, i * span + stride)],
                data.at[0, pl.ds(pl.multiple_of(rank * stride, 16), stride)],
                to,
            )
        )
        go(
            z_copy(
                1, i, rank,
                z_send.at[slice(i * span + stride, (i + 1) * span)],
                z_extra.at[rank],
                to,
            )
        )
    own = contract(spread[block(0), :], normed, NN).astype(bf)
    data[0, chunk(0), :] = own[:stride]
    z_extra[0] = own[stride:]

    flows = []
    for o in range(GROUPS):
        ch = chunk(o)
        flows.append(
            dict(
                a_y=copy(data.at[0, ch, left], data.at[2, ch, left], along),
                b_x=copy(data.at[0, ch, right], data.at[4, ch, right], across),
                a_x=copy(data.at[0, ch, left], data.at[4, ch, left], across),
                b_y=copy(data.at[0, ch, right], data.at[2, ch, right], along),
                c_0=copy(data.at[0, ch], data.at[1, ch], core),
                a_d=copy(data.at[2, ch, left], data.at[6, ch, left], across),
                b_d=copy(data.at[4, ch, right], data.at[6, ch, right], along),
                c_y=copy(data.at[2, ch], data.at[3, ch], core),
                c_x=copy(data.at[4, ch], data.at[5, ch], core),
                c_d=copy(data.at[6, ch], data.at[7, ch], core),
                h_y=copy(hid.at[slice(2, 4), ch], hgot.at[0, :, ch], along),
                h_x=copy(hid.at[slice(4, 6), ch], hgot.at[1, :, ch], across),
                h_d=copy(hid.at[slice(6, 8), ch], hgot.at[2, :, ch], corner),
                p_c=copy(part.at[ch], pgot.at[ch], core),
            )
        )

    def arrive(kind, o, target):
        z_copy(kind, 0, o, target, target, core).wait_recv()

    def stage(o):
        flow = flows[o]
        if o:
            arrive(0, o, data.at[0, slice(o * stride, (o + 1) * stride)])
        if o == GROUPS - 1:
            more = z_extra[0].astype(f32)
            for k in range(1, GROUPS):
                arrive(1, k, z_extra.at[k])
                more = more + z_extra[k].astype(f32)
            data[0, GROUPS * stride :, :] = more.astype(bf)
        for name in ("a_y", "b_x", "a_x", "b_y", "c_0"):
            go(flow[name])

    def forward(o):
        flow = flows[o]
        flow["a_y"].wait_recv()
        go(flow["a_d"])
        flow["b_x"].wait_recv()
        go(flow["b_d"])
        flow["b_y"].wait_recv()
        go(flow["c_y"])
        flow["a_x"].wait_recv()
        go(flow["c_x"])

    def finish(o):
        flow = flows[o]
        flow["a_d"].wait_recv()
        flow["b_d"].wait_recv()
        go(flow["c_d"])

    def compute(o):
        flow, ch = flows[o], chunk(o)
        for name in ("c_0", "c_y", "c_x", "c_d"):
            flow[name].wait_recv()
        n = ch.stop - ch.start

        @pl.loop(0, 2)
        def _(m):
            some = pl.ds(m * 4, 4)
            x = data[some, ch, :].reshape(4 * n, width)
            gate = contract(x, v_gate[...], NN)
            up = contract(x, v_up[...], NN)
            hidden = (gate / (1.0 + jnp.exp(-gate)) * up).astype(bf)
            hid[some, ch, :] = hidden.reshape(4, n, units)

        for name in ("h_y", "h_x", "h_d"):
            go(flow[name])

    lane = lax.broadcasted_iota(jnp.int32, (1, 128), 1)

    def down(o):
        flow, ch = flows[o], chunk(o)
        n = ch.stop - ch.start
        w = wslot[:, ch, :].reshape(2 * n, 128).astype(f32)
        pick = lambda s: jnp.sum(
            jnp.where((lane == s) | (lane == s + 64), w, 0.0), axis=1, keepdims=True
        )
        mine, other = pick(side), pick(1 - side)
        for name in ("h_y", "h_x", "h_d"):
            flow[name].wait_recv()
        tile = 512

        @pl.loop(0, width // tile)
        def _(j):
            cols = pl.ds(pl.multiple_of(j * tile, tile), tile)
            rows = lambda value: value.reshape(2 * n, units)
            a = contract(rows(hid[0:2, ch, :]), wd[0, :, cols], NN) + contract(
                rows(hgot[1, :, ch, :]), wd[2, :, cols], NN
            )
            b = contract(rows(hgot[0, :, ch, :]), wd[1, :, cols], NN) + contract(
                rows(hgot[2, :, ch, :]), wd[3, :, cols], NN
            )
            value = a * mine + b * other
            acc[ch, cols] = value[:n]
            part[ch, cols] = value[n:].astype(bf)

        go(flow["p_c"])

    def give(o):
        flow, ch = flows[o], chunk(o)
        flow["p_c"].wait_recv()
        outs[ch, :] = (acc[ch, :] + pgot[ch, :].astype(f32)).astype(bf)
        rows = slice(o * stride, (o + 1) * stride)
        if o == 0:
            back_got[0:stride] = outs[rows, :]
        else:
            i, rank, to = far[o - 1]
            go(
                z_copy(
                    2, i, rank,
                    outs.at[rows],
                    back_got.at[pl.ds(pl.multiple_of(rank * span, 16), stride)],
                    to,
                )
            )
        if o == GROUPS - 1:
            rows = slice(GROUPS * stride, length)
            back_got[stride:span] = outs[rows, :]
            for i, rank, to in far:
                go(
                    z_copy(
                        3, i, rank,
                        outs.at[rows],
                        back_got.at[pl.ds(pl.multiple_of(rank * span + stride, 16), extra)],
                        to,
                    )
                )

    stage(0)
    down_y[0].wait_recv()
    down_y[1].wait_recv()
    go(down_yx)
    down_x.wait_recv()
    go(down_xy)
    forward(0)
    stage(1)
    for load in loads:
        load.wait()
    meta_core.wait_recv()
    finish(0)
    forward(1)
    compute(0)
    finish(1)
    stage(2)
    down_yx.wait_recv()
    down_xy.wait_recv()
    down(0)
    compute(1)
    give(0)
    forward(2)
    down(1)
    stage(3)
    finish(2)
    give(1)
    compute(2)
    forward(3)
    down(2)
    finish(3)
    give(2)
    compute(3)
    down(3)
    give(3)
    for i in range(1, GROUPS):
        arrive(2, i, back_got.at[slice(i * span, i * span + stride)])
        arrive(3, i, back_got.at[slice(i * span + stride, (i + 1) * span)])
    picked = contract(spread[...], back_got[...], TN)
    out_ref[...] = (kept[...].astype(f32) + picked).astype(bf)
    for one in pending + started:
        one.wait_send()


def whole_layer(n_sp, n_tp, args, residual, norm_gain, routes, weights, capacity, w_gate, w_up, w_down):
    rows, width = residual.shape
    units = w_gate.shape[1]
    stride = capacity // 16 * 16
    over = capacity - stride
    extra = max(16, -(-GROUPS * over // 16) * 16)
    span, length = stride + extra, GROUPS * stride + extra
    place = lax.axis_index("sp") // 2
    group = routes[:, 0] // 2
    position = jnp.arange(rows, dtype=jnp.int32)
    before = (group[:, None] == group[None, :]) & (position[None, :] < position[:, None])
    nth = jnp.sum(before.astype(jnp.int32), axis=1)
    tail = stride + rank_of(group, place) * over + nth - stride
    slot = (rank_of(place, group) * span + jnp.where(nth < stride, nth, tail))[None, :]
    side = routes[:, :, None] % 2 == (jnp.arange(128, dtype=jnp.int32) % 64)[None, None, :]
    weight = jnp.sum(jnp.where(side, weights[:, :, None], 0.0), axis=1)
    bf, f32 = jnp.bfloat16, jnp.float32
    vmem = pl.BlockSpec(memory_space=pltpu.VMEM)
    hbm = pl.BlockSpec(memory_space=pl.ANY)
    sem = pltpu.SemaphoreType.DMA
    mine = mix_scratch(n_sp, n_tp, args, residual)
    return pl.pallas_call(
        functools.partial(layer_kernel, n_sp, n_tp, stride, extra, len(mine)),
        out_shape=jax.ShapeDtypeStruct((rows, width), bf),
        in_specs=[vmem] * 18 + [hbm] * 3,
        out_specs=vmem,
        scratch_shapes=mine
        + [
            pltpu.VMEM(w_gate.shape, bf),
            pltpu.VMEM(w_up.shape, bf),
            pltpu.VMEM((4, units, width), bf),
            pltpu.VMEM((GROUPS * span, rows), bf),
            pltpu.VMEM((GROUPS * span, 128), bf),
            pltpu.VMEM((GROUPS, span, 128), bf),
            pltpu.VMEM((2, length, 128), bf),
            pltpu.VMEM((GROUPS * span, width), bf),
            pltpu.VMEM((GROUPS, extra, width), bf),
            pltpu.VMEM((8, length, width), bf),
            pltpu.VMEM((8, length, units), bf),
            pltpu.VMEM((3, 2, length, units), bf),
            pltpu.VMEM((length, width), f32),
            pltpu.VMEM((length, width), bf),
            pltpu.VMEM((length, width), bf),
            pltpu.VMEM((length, width), bf),
            pltpu.VMEM((GROUPS * span, width), bf),
            pltpu.VMEM((rows, width), bf),
            sem((3,)),
            sem((COPIES,)),
            sem((COPIES,)),
            sem((KINDS * GROUPS,)),
            sem((KINDS * GROUPS,)),
        ],
        compiler_params=pltpu.CompilerParams(
            collective_id=1, has_side_effects=True, vmem_limit_bytes=63 * 2**20
        ),
    )(*mix_operands(args, residual, norm_gain), weight, slot, w_gate, w_up, w_down)


def slot_table(routes, capacity, experts):
    flat = routes.reshape(-1)
    count = flat.shape[0]
    onehot = (flat[:, None] == jnp.arange(experts, dtype=jnp.int32)[None, :]).astype(jnp.int32)
    place = jnp.sum((jnp.cumsum(onehot, axis=0) - onehot) * onehot, axis=1)
    table = (
        jnp.full((experts, capacity), count, jnp.int32)
        .at[flat, place]
        .set(jnp.arange(count, dtype=jnp.int32))
    )
    return (table, place)

def body(
    residual,
    query_one,
    key_one,
    value_one,
    gate_one,
    decay_one,
    norm_one,
    output_one,
    query_two,
    key_two,
    value_two,
    gate_two,
    decay_two,
    norm_two,
    output_two,
    norm_gain,
    expert_ids,
    group_weight,
    pair_weight,
    expert_gate,
    expert_up,
    expert_down,
):
    n_sp, n_tp = lax.axis_size("sp"), lax.axis_size("tp")
    mixing = (
        query_one, key_one, value_one, gate_one, decay_one, norm_one, output_one,
        query_two, key_two, value_two, gate_two, decay_two, norm_two, output_two,
    )
    rows_dev = residual.shape[0]
    rank = lax.axis_index("tp")
    experts = n_sp
    capacity = max(2, 2 * rows_dev // (experts - GROUPS) + 1)
    own_routes = lax.dynamic_slice_in_dim(expert_ids, rank * rows_dev, rows_dev, 0)
    own_group = lax.dynamic_slice_in_dim(group_weight, rank * rows_dev, rows_dev, 0)
    own_pair = lax.dynamic_slice_in_dim(pair_weight, rank * rows_dev, rows_dev, 0)
    weights = own_group[:, None] * own_pair / jnp.sum(own_pair, axis=1, keepdims=True)
    if experts == 2 * GROUPS and n_tp == 4:
        return whole_layer(
            n_sp,
            n_tp,
            mixing,
            residual,
            norm_gain,
            own_routes,
            weights,
            capacity,
            expert_gate[0],
            expert_up[0],
            expert_down[0],
        )
    stream, normed_rows = mixer(n_sp, n_tp, mixing, residual, norm_gain)
    blank = jnp.zeros((1, D), jnp.bfloat16)
    table, own_place = slot_table(own_routes, capacity, experts)
    index = jnp.where(table == 2 * rows_dev, rows_dev, table // 2)
    send = jnp.concatenate([normed_rows, blank], axis=0)[index][None]
    received = lax.all_to_all(send, "sp", split_axis=1, concat_axis=1, tiled=True)
    received = lax.all_gather(received, "tp", axis=0, tiled=True)
    flat = received.reshape(-1, received.shape[-1])
    gate_part = jnp.dot(flat, expert_gate[0], preferred_element_type=jnp.float32)
    up_part = jnp.dot(flat, expert_up[0], preferred_element_type=jnp.float32)
    hidden = (jax.nn.silu(gate_part) * up_part).astype(jnp.bfloat16)
    share_sum = lax.psum_scatter(
        jnp.dot(hidden, expert_down[0], preferred_element_type=jnp.float32)
        .reshape(received.shape)
        .astype(jnp.bfloat16),
        "tp",
        scatter_dimension=0,
        tiled=True,
    )
    returned = lax.all_to_all(share_sum, "sp", split_axis=1, concat_axis=1, tiled=True)
    slot_index = own_routes.reshape(-1) * capacity + own_place
    picked = returned.reshape(-1, D)[slot_index].astype(jnp.float32).reshape(rows_dev, 2, D)
    layer = stream.astype(jnp.float32) + jnp.sum(weights[:, :, None] * picked, axis=1)
    return layer.astype(jnp.bfloat16)

def solution(mesh):
    placed = (
        P(("sp", "tp"), None),
        P("sp", "tp"),
        P("sp", "tp"),
        P("sp", "tp"),
        P("sp", "tp"),
        P(None, "sp", "tp"),
        P(),
        P("tp", None),
        P("sp", "tp"),
        P("sp", "tp"),
        P("sp", "tp"),
        P("sp", "tp"),
        P(None, "sp", "tp"),
        P(),
        P("tp", None),
        P(),
        P("sp", None),
        P("sp"),
        P("sp", None),
        P("sp", None, "tp"),
        P("sp", None, "tp"),
        P("sp", "tp", None),
    )
    return jax.shard_map(
        body, mesh=mesh, in_specs=placed, out_specs=P(("sp", "tp"), None), check_vma=False
    )
```

time: 164 us -> 131 us (0.80); the launches traced: 161 us -> 131 us
  Pallas kernels: 156 us -> 126 us
    pallas_call x2 -> x1, Pallas kernels: 156 us -> 126 us  [whole_layer(): pl.pallas_call(functools.partial(layer_kernel, n_sp, n_tp, stride, extra,...]
where the time goes in v1:
time: 131 us
  Pallas kernels  126 us (96%)
  local copies, waits for them, and re-layouts  2.54 us (2%)
  other arithmetic  2.48 us (2%)
    pallas_call x1, Pallas kernels, whole_layer(): pl.pallas_call(functools.partial(layer_kernel, n_sp, n_tp, stride, extra,...  126 us

profile of v1, /device:TPU:0, one launch (start us, length us, event | category | flops | bytes accessed | tf_op | source)
XLA Modules:
  0.0 130.6 jit_solution(13007613780243884167)
XLA Ops:
  0.0 0.0 copy-start
  0.0 0.8 dynamic_slice.10
  0.8 0.0 copy-done
  0.8 0.1 dynamic-slice_reduce_fusion
  0.9 0.1 multiply_divide_fusion
  0.9 0.8 and_select_fusion.7
  1.7 0.2 convert_reduce_fusion
  1.9 0.6 fusion.2.refs_17_
  2.5 0.7 select_reduce_fusion.refs_16_
  3.3 125.6 %shard_map.208 = bf16[96,2048]{1,0:T(8,128)(2,1)} custom-call(bf16[384,128]{1,0:T(8,128)(2,1)} %refs_0_.1, bf16[384,128]{1,0:T(8,128)(2,1)} %refs_1_.1, bf16[384,256]{1,0:T(8,128)(2,1)} %refs_2_.1, bf16[384,256]{1,0:T(8,128)(2,1)} %refs_3_.1, bf16[2,384,128]{2,1,0:T(8,128)(2,1)} %refs_4_.1, bf16[384,256]{1,0:T(8,128)(2,1)} %refs_5_.1, ...), custom_call_target="tpu_custom_call" | custom-call | tf_op jit(solution)/shard_map/pallas_call | solution.py:675
  128.8 1.8 %copy.26 = bf16[96,2048]{1,0:T(8,128)(2,1)} copy(bf16[96,2048]{1,0:T(8,128)(2,1)} %shard_map.208) | data formatting | bytes 786432
  (3 shorter events, 0.0 us)
Async XLA Ops:
  0.0 0.8 copy-start

commit v2 on v1

--- a/solution.py
+++ b/solution.py
@@ -63,7 +63,8 @@
 def mix(n_sp, n_tp, operands, scratch, ready, sent_states, got_states):
     q1, k1, v1, g1, d1, q2, k2, v2, g2, d2, norm1, norm2, out1, out2, res, gain = operands
     cum, qd, kd, added, ends, sent, got, carried, total, mixed, part_send, part_got = scratch[:12]
-    st_send, st_recv, pt_send, pt_recv = scratch[12:]
+    fade_own, fade_all, half_send, half_got = scratch[12:16]
+    st_send, st_recv, pt_send, pt_recv, fd_send, fd_recv, hf_send, hf_recv = scratch[16:]
     sp, tp = lax.axis_index("sp"), lax.axis_index("tp")
     length = q1.shape[0]
     blocks = length // BLOCK
@@ -78,6 +79,9 @@
             units.append((q, k, v, g, d, norm, key, per, at))
     count = len(units)
     bits = [1 << r for r in range(n_tp.bit_length() - 1)]
+    paired = n_sp == 2 * GROUPS
+    place, side = sp // 2, lax.rem(sp, 2)
+    mate = (flip_bit(sp, 1), tp)
 
     meet(
         [(lax.rem(sp + off, n_sp), tp) for off in range(1, n_sp)]
@@ -94,6 +98,26 @@
         return remote(
             sent.at[way, rows], got.at[off, rows], st_send.at[sem], st_recv.at[sem], (to, tp)
         )
+
+    def place_copy(u, off):
+        z = lax.rem(place + off, GROUPS)
+        way = jnp.where(z > place, 0, 1) if off else side
+        rows = slice(u * PACK, u * PACK + VALUE_W)
+        sem = off * count + u
+        return remote(
+            sent.at[way, rows],
+            got.at[off, rows],
+            st_send.at[sem],
+            st_recv.at[sem],
+            (z * 2 + side, tp) if off else mate,
+        )
+
+    def fade_copy(off):
+        to = (lax.rem(sp + off, n_sp), tp)
+        return remote(fade_own, fade_all.at[off], fd_send.at[off], fd_recv.at[off], to)
+
+    def half_copy(u):
+        return remote(half_send.at[u], half_got.at[u], hf_send.at[u], hf_recv.at[u], mate)
 
     t_at = lax.broadcasted_iota(jnp.int32, (length, length), 0)
     s_at = lax.broadcasted_iota(jnp.int32, (length, length), 1)
@@ -134,13 +158,28 @@
                 state = state * fade + term
                 reach = reach + e
             sent[way, u * PACK : u * PACK + VALUE_W, :] = state.astype(jnp.bfloat16)
-            sent[way, u * PACK + VALUE_W : (u + 1) * PACK, :] = jnp.broadcast_to(
-                jnp.exp(reach), (16, lanes)
-            ).astype(jnp.bfloat16)
+            if paired:
+                row = way * count + u
+                fade_own[row : row + 1, :] = jnp.exp(reach)
+            else:
+                sent[way, u * PACK + VALUE_W : (u + 1) * PACK, :] = jnp.broadcast_to(
+                    jnp.exp(reach), (16, lanes)
+                ).astype(jnp.bfloat16)
+
+        if paired:
+            for off in (1, 2, 3, 0):
+                place_copy(u, off).start()
+        else:
+
+            @pl.loop(1, n_sp)
+            def _(off):
+                state_copy(u, off).start()
+
+    if paired:
 
         @pl.loop(1, n_sp)
         def _(off):
-            state_copy(u, off).start()
+            fade_copy(off).start()
 
     sent_states()
     t_blk = lax.broadcasted_iota(jnp.int32, (BLOCK, BLOCK), 0)
@@ -164,12 +203,6 @@
                 total[first + h, rows, :] = contract(scores.astype(jnp.bfloat16), value, NN)
         first += per
 
-    @pl.loop(1, n_sp)
-    def _(off):
-        for u in range(count):
-            state_copy(u, off).wait()
-
-    got_states()
     carried[...] = jnp.zeros_like(carried)
 
     def fold(way, who):
@@ -179,13 +212,61 @@
             state = got[off, u * PACK : u * PACK + VALUE_W, :]
             carried[way, u] = carried[way, u] * fade.astype(jnp.float32) + state.astype(jnp.float32)
 
-    @pl.loop(0, sp)
-    def _(who):
-        fold(0, who)
-
-    @pl.loop(0, n_sp - 1 - sp)
-    def _(back):
-        fold(1, n_sp - 1 - back)
+    def fade_of(who, way, u):
+        row = way * count + u
+        return fade_all[lax.rem(sp - who + n_sp, n_sp), row : row + 1, :]
+
+    def fold_place(way, u, z):
+        off = lax.rem(place - z + GROUPS, GROUPS)
+        fades = [fade_of(2 * z + y, way, u) for y in range(2)]
+        state = got[off, u * PACK : u * PACK + VALUE_W, :].astype(jnp.float32)
+        later = jnp.where(side == way, fades[1 - way], jnp.ones_like(fades[0]))
+        carried[way, u] = carried[way, u] * (fades[0] * fades[1]) + state * later
+
+    if paired:
+
+        @pl.loop(1, n_sp)
+        def _(off):
+            fade_copy(off).wait()
+
+        for u in range(count):
+            for off in range(1, GROUPS):
+                place_copy(u, off).wait()
+
+            @pl.loop(0, place)
+            def _(z):
+                fold_place(0, u, z)
+
+            @pl.loop(0, GROUPS - 1 - place)
+            def _(back):
+                fold_place(1, u, GROUPS - 1 - back)
+
+            half_send[u] = carried[:, u].astype(jnp.bfloat16)
+            half_copy(u).start()
+        got_states()
+        for u in range(count):
+            place_copy(u, 0).wait()
+            half_copy(u).wait()
+            carried[:, u] = carried[:, u] + half_got[u].astype(jnp.float32)
+            way = 1 - side
+            off = 1 + way * (n_sp - 2)
+            fade = fade_all[off, pl.ds(way * count + u, 1), :]
+            state = got[0, u * PACK : u * PACK + VALUE_W, :].astype(jnp.float32)
+            carried[way, u] = carried[way, u] * fade + state
+    else:
+
+        @pl.loop(1, n_sp)
+        def _(off):
+            for u in range(count):
+                state_copy(u, off).wait()
+
+        @pl.loop(0, sp)
+        def _(who):
+            fold(0, who)
+
+        @pl.loop(0, n_sp - 1 - sp)
+        def _(back):
+            fold(1, n_sp - 1 - back)
 
     first = 0
     for u, (q, k, v, g, d, norm, key, per, at) in enumerate(units):
@@ -280,10 +361,18 @@
         pltpu.VMEM((length, heads * VALUE_W), bf),
         pltpu.VMEM((n_tp, rows, width), bf),
         pltpu.VMEM((n_tp, rows, width), bf),
+        pltpu.VMEM((-(-2 * count // 8) * 8, 128), f32),
+        pltpu.VMEM((n_sp, -(-2 * count // 8) * 8, 128), f32),
+        pltpu.VMEM((count, 2, VALUE_W, 128), bf),
+        pltpu.VMEM((count, 2, VALUE_W, 128), bf),
         sem((n_sp * count,)),
         sem((n_sp * count,)),
         sem((n_tp,)),
         sem((n_tp,)),
+        sem((n_sp,)),
+        sem((n_sp,)),
+        sem((count,)),
+        sem((count,)),
     ]
 
 
@@ -342,18 +431,19 @@
 COPIES = 10 * GROUPS + 4 * GROUPS + 8
 
 
-def layer_kernel(n_sp, n_tp, stride, extra, n_scratch, *refs):
+def layer_kernel(n_sp, n_tp, stride, over, extra, n_scratch, *refs):
     operands = refs[:16]
-    weight, slot, w_gate, w_up, w_down, out_ref = refs[16:22]
-    scratch = refs[22 : 22 + n_scratch]
+    ids, group_share, pair_share, w_gate, w_up, w_down, out_ref = refs[16:23]
+    scratch = refs[23 : 23 + n_scratch]
     (
         v_gate, v_up, wd, spread, meta_send, meta_got, wslot, z_send, z_extra, data, hid, hgot,
         acc, part, pgot, outs, back_got, kept, w_sem, s_sem, r_sem, zs_sem, zr_sem,
-    ) = refs[22 + n_scratch :]
+    ) = refs[23 + n_scratch :]
     bf, f32 = jnp.bfloat16, jnp.float32
     sp, tp = lax.axis_index("sp"), lax.axis_index("tp")
     span = stride + extra
     length = GROUPS * stride + extra
+    wire = -(-GROUPS * over // 8) * 8
     width = data.shape[2]
     units = hid.shape[2]
     place, side = sp // 2, lax.rem(sp, 2)
@@ -391,7 +481,7 @@
             ((w_gate, v_gate), (w_up, v_up), (w_down, wd.at[0]))
         )
     ]
-    early = units // 4
+    early = units // 2
     down_y = [
         copy(w_down.at[rows], wd.at[1, rows], along)
         for rows in (slice(0, early), slice(early, units))
@@ -412,24 +502,63 @@
     def chunk(o):
         return slice(o * stride, (o + 1) * stride if o < GROUPS - 1 else length)
 
+    def moved(o):
+        return slice(o * stride, (o + 1) * stride if o < GROUPS - 1 else GROUPS * stride + wire)
+
+    def routing():
+        rows, tokens = spread.shape[1], ids.shape[1]
+        first, share = ids[0:1, :], group_share[...]
+        kind = lax.broadcasted_iota(jnp.int32, (8, 1), 0)
+        member = ((first >= 2 * kind) & (first < 2 * kind + 2)).astype(f32)
+        from_at = lax.broadcasted_iota(jnp.int32, (tokens, tokens), 0)
+        to_at = lax.broadcasted_iota(jnp.int32, (tokens, tokens), 1)
+        before = jnp.where((from_at < to_at) & (from_at // rows == to_at // rows), 1.0, 0.0)
+        counts = contract(member.astype(bf), before.astype(bf), NN)
+        nth = jnp.sum(member * counts, axis=0, keepdims=True)
+        named = lax.rem(kind, GROUPS)
+        base = (rank_of(place, named) * span).astype(f32)
+        shift = (rank_of(named, place) * over).astype(f32)
+        seat = base + jnp.where(nth < stride, nth, nth + shift)
+        seat = jnp.sum(member * seat, axis=0, keepdims=True)
+        pair = pair_share[0:1, :] + pair_share[1:2, :]
+        w_first = share * pair_share[0:1, :] / pair
+        w_second = share * pair_share[1:2, :] / pair
+        even = lax.rem(first, 2) == 0
+        table = jnp.zeros((8, tokens), f32)
+        table = jnp.where(kind == 0, seat, table)
+        for s in range(2):
+            w = jnp.where(even, w_first, w_second) if s == 0 else jnp.where(even, w_second, w_first)
+            high = w.astype(bf).astype(f32)
+            table = jnp.where(kind == 1 + s, high, table)
+            table = jnp.where(kind == 3 + s, w - high, table)
+        at = lax.broadcasted_iota(jnp.int32, (tokens, rows), 0)
+        own_at = lax.broadcasted_iota(jnp.int32, (tokens, rows), 1) + tp * rows
+        select = jnp.where(at == own_at, 1.0, 0.0).astype(bf)
+        table = contract(table.astype(bf), select, NN)
+        seats = lax.broadcasted_iota(jnp.int32, (GROUPS * span, rows), 0)
+        spread[...] = jnp.where(seats == table[0:1].astype(jnp.int32), 1.0, 0.0).astype(bf)
+        line = lax.broadcasted_iota(jnp.int32, (128, 1), 0)
+        lines = jnp.zeros((128, rows), f32)
+        for row, spot in ((1, 0), (2, 1), (3, 64), (4, 65)):
+            lines = jnp.where(line == spot, table[row : row + 1], lines)
+        meta_send[...] = contract(spread[...], lines.astype(bf), NT).astype(bf)
+
     def ready(begin):
         if begin is None:
-            return [core_peer for core_peer in (corner,)]
+            return [corner]
         for load in loads:
             load.start()
+        rest = slice(GROUPS * stride + wire, length)
+        if wire < extra:
+            data[:, rest, :] = jnp.zeros((8, extra - wire, width), bf)
+            hgot[:, :, rest, :] = jnp.zeros((3, 2, extra - wire, units), bf)
+            pgot[rest, :] = jnp.zeros((extra - wire, width), bf)
+            for i in range(GROUPS):
+                spare = slice(i * span + stride + wire, (i + 1) * span)
+                back_got[spare, :] = jnp.zeros((extra - wire, width), bf)
         go(down_x)
         go(down_y[0])
-        rows = slot.shape[1]
-        spread[...] = (
-            (lax.broadcasted_iota(jnp.int32, (GROUPS * span, rows), 0) == slot[...])
-            .astype(f32)
-            .astype(bf)
-        )
-        high = weight[...].astype(bf)
-        rest = (weight[...] - high.astype(f32)).astype(bf)
-        second = lax.broadcasted_iota(jnp.int32, high.shape, 1) >= 64
-        both = jnp.where(second, rest.astype(f32), high.astype(f32)).astype(bf)
-        meta_send[...] = contract(spread[...], both, NN).astype(bf)
+        routing()
         for one in metas:
             go(one)
 
@@ -466,18 +595,18 @@
         go(
             z_copy(
                 1, i, rank,
-                z_send.at[slice(i * span + stride, (i + 1) * span)],
+                z_send.at[slice(i * span + stride, i * span + stride + wire)],
                 z_extra.at[rank],
                 to,
             )
         )
     own = contract(spread[block(0), :], normed, NN).astype(bf)
     data[0, chunk(0), :] = own[:stride]
-    z_extra[0] = own[stride:]
+    z_extra[0] = own[stride : stride + wire]
 
     flows = []
     for o in range(GROUPS):
-        ch = chunk(o)
+        ch = moved(o)
         flows.append(
             dict(
                 a_y=copy(data.at[0, ch, left], data.at[2, ch, left], along),
@@ -509,7 +638,7 @@
             for k in range(1, GROUPS):
                 arrive(1, k, z_extra.at[k])
                 more = more + z_extra[k].astype(f32)
-            data[0, GROUPS * stride :, :] = more.astype(bf)
+            data[0, GROUPS * stride : GROUPS * stride + wire, :] = more.astype(bf)
         for name in ("a_y", "b_x", "a_x", "b_y", "c_0"):
             go(flow[name])
 
@@ -596,86 +725,77 @@
                 )
             )
         if o == GROUPS - 1:
-            rows = slice(GROUPS * stride, length)
-            back_got[stride:span] = outs[rows, :]
+            rows = slice(GROUPS * stride, GROUPS * stride + wire)
+            back_got[stride : stride + wire] = outs[rows, :]
             for i, rank, to in far:
                 go(
                     z_copy(
                         3, i, rank,
                         outs.at[rows],
-                        back_got.at[pl.ds(pl.multiple_of(rank * span + stride, 16), extra)],
+                        back_got.at[pl.ds(pl.multiple_of(rank * span + stride, 16), wire)],
                         to,
                     )
                 )
 
     stage(0)
+    forward(0)
+    stage(1)
+    for load in loads:
+        load.wait()
+    finish(0)
+    compute(0)
+    forward(1)
     down_y[0].wait_recv()
     down_y[1].wait_recv()
     go(down_yx)
     down_x.wait_recv()
     go(down_xy)
-    forward(0)
-    stage(1)
-    for load in loads:
-        load.wait()
+    stage(2)
+    finish(1)
+    compute(1)
+    forward(2)
+    stage(3)
     meta_core.wait_recv()
-    finish(0)
-    forward(1)
-    compute(0)
-    finish(1)
-    stage(2)
     down_yx.wait_recv()
     down_xy.wait_recv()
     down(0)
-    compute(1)
+    finish(2)
+    compute(2)
+    down(1)
+    forward(3)
     give(0)
-    forward(2)
-    down(1)
-    stage(3)
-    finish(2)
     give(1)
-    compute(2)
-    forward(3)
     down(2)
     finish(3)
+    compute(3)
     give(2)
-    compute(3)
     down(3)
     give(3)
     for i in range(1, GROUPS):
         arrive(2, i, back_got.at[slice(i * span, i * span + stride)])
-        arrive(3, i, back_got.at[slice(i * span + stride, (i + 1) * span)])
+        arrive(3, i, back_got.at[slice(i * span + stride, i * span + stride + wire)])
     picked = contract(spread[...], back_got[...], TN)
     out_ref[...] = (kept[...].astype(f32) + picked).astype(bf)
     for one in pending + started:
         one.wait_send()
 
 
-def whole_layer(n_sp, n_tp, args, residual, norm_gain, routes, weights, capacity, w_gate, w_up, w_down):
+def whole_layer(n_sp, n_tp, args, residual, norm_gain, routing, capacity, w_gate, w_up, w_down):
     rows, width = residual.shape
     units = w_gate.shape[1]
     stride = capacity // 16 * 16
     over = capacity - stride
     extra = max(16, -(-GROUPS * over // 16) * 16)
     span, length = stride + extra, GROUPS * stride + extra
-    place = lax.axis_index("sp") // 2
-    group = routes[:, 0] // 2
-    position = jnp.arange(rows, dtype=jnp.int32)
-    before = (group[:, None] == group[None, :]) & (position[None, :] < position[:, None])
-    nth = jnp.sum(before.astype(jnp.int32), axis=1)
-    tail = stride + rank_of(group, place) * over + nth - stride
-    slot = (rank_of(place, group) * span + jnp.where(nth < stride, nth, tail))[None, :]
-    side = routes[:, :, None] % 2 == (jnp.arange(128, dtype=jnp.int32) % 64)[None, None, :]
-    weight = jnp.sum(jnp.where(side, weights[:, :, None], 0.0), axis=1)
     bf, f32 = jnp.bfloat16, jnp.float32
     vmem = pl.BlockSpec(memory_space=pltpu.VMEM)
     hbm = pl.BlockSpec(memory_space=pl.ANY)
     sem = pltpu.SemaphoreType.DMA
     mine = mix_scratch(n_sp, n_tp, args, residual)
     return pl.pallas_call(
-        functools.partial(layer_kernel, n_sp, n_tp, stride, extra, len(mine)),
+        functools.partial(layer_kernel, n_sp, n_tp, stride, over, extra, len(mine)),
         out_shape=jax.ShapeDtypeStruct((rows, width), bf),
-        in_specs=[vmem] * 18 + [hbm] * 3,
+        in_specs=[vmem] * 19 + [hbm] * 3,
         out_specs=vmem,
         scratch_shapes=mine
         + [
@@ -687,7 +807,7 @@
             pltpu.VMEM((GROUPS, span, 128), bf),
             pltpu.VMEM((2, length, 128), bf),
             pltpu.VMEM((GROUPS * span, width), bf),
-            pltpu.VMEM((GROUPS, extra, width), bf),
+            pltpu.VMEM((GROUPS, -(-GROUPS * over // 8) * 8, width), bf),
             pltpu.VMEM((8, length, width), bf),
             pltpu.VMEM((8, length, units), bf),
             pltpu.VMEM((3, 2, length, units), bf),
@@ -706,7 +826,7 @@
         compiler_params=pltpu.CompilerParams(
             collective_id=1, has_side_effects=True, vmem_limit_bytes=63 * 2**20
         ),
-    )(*mix_operands(args, residual, norm_gain), weight, slot, w_gate, w_up, w_down)
+    )(*mix_operands(args, residual, norm_gain), *routing, w_gate, w_up, w_down)
 
 
 def slot_table(routes, capacity, experts):
@@ -754,10 +874,6 @@
     rank = lax.axis_index("tp")
     experts = n_sp
     capacity = max(2, 2 * rows_dev // (experts - GROUPS) + 1)
-    own_routes = lax.dynamic_slice_in_dim(expert_ids, rank * rows_dev, rows_dev, 0)
-    own_group = lax.dynamic_slice_in_dim(group_weight, rank * rows_dev, rows_dev, 0)
-    own_pair = lax.dynamic_slice_in_dim(pair_weight, rank * rows_dev, rows_dev, 0)
-    weights = own_group[:, None] * own_pair / jnp.sum(own_pair, axis=1, keepdims=True)
     if experts == 2 * GROUPS and n_tp == 4:
         return whole_layer(
             n_sp,
@@ -765,13 +881,16 @@
             mixing,
             residual,
             norm_gain,
-            own_routes,
-            weights,
+            (expert_ids.T, group_weight[None], pair_weight.T),
             capacity,
             expert_gate[0],
             expert_up[0],
             expert_down[0],
         )
+    own_routes = lax.dynamic_slice_in_dim(expert_ids, rank * rows_dev, rows_dev, 0)
+    own_group = lax.dynamic_slice_in_dim(group_weight, rank * rows_dev, rows_dev, 0)
+    own_pair = lax.dynamic_slice_in_dim(pair_weight, rank * rows_dev, rows_dev, 0)
+    weights = own_group[:, None] * own_pair / jnp.sum(own_pair, axis=1, keepdims=True)
     stream, normed_rows = mixer(n_sp, n_tp, mixing, residual, norm_gain)
     blank = jnp.zeros((1, D), jnp.bfloat16)
     table, own_place = slot_table(own_routes, capacity, experts)

time: 131 us -> 131 us (level)
  other arithmetic: 2.48 us -> 0 us
  Pallas kernels: 126 us -> 128 us
    pallas_call x1, Pallas kernels: 126 us -> 128 us  [whole_layer(): pl.pallas_call(functools.partial(layer_kernel, n_sp, n_tp, stride, over,...]
where the time goes in v2:
time: 131 us
  Pallas kernels  128 us (98%)
  local copies, waits for them, and re-layouts  3.01 us (2%)
    pallas_call x1, Pallas kernels, whole_layer(): pl.pallas_call(functools.partial(layer_kernel, n_sp, n_tp, stride, over,...  128 us

profile of v2, /device:TPU:0, one launch (start us, length us, event | category | flops | bytes accessed | tf_op | source)
XLA Modules:
  0.0 131.3 jit_solution(6254247068125253326)
XLA Ops:
  0.0 0.0 copy-start
  0.0 0.7 copy-done
  0.7 0.6 broadcast_in_dim.15.refs_17_
  1.2 128.2 %shard_map.208 = bf16[96,2048]{1,0:T(8,128)(2,1)} custom-call(bf16[384,128]{1,0:T(8,128)(2,1)} %refs_0_.1, bf16[384,128]{1,0:T(8,128)(2,1)} %refs_1_.1, bf16[384,256]{1,0:T(8,128)(2,1)} %refs_2_.1, bf16[384,256]{1,0:T(8,128)(2,1)} %refs_3_.1, bf16[2,384,128]{2,1,0:T(8,128)(2,1)} %refs_4_.1, bf16[384,256]{1,0:T(8,128)(2,1)} %refs_5_.1, ...), custom_call_target="tpu_custom_call" | custom-call | tf_op jit(solution)/shard_map/pallas_call | solution.py:795
  129.5 1.8 %copy.24 = bf16[96,2048]{1,0:T(8,128)(2,1)} copy(bf16[96,2048]{1,0:T(8,128)(2,1)} %shard_map.208) | data formatting | bytes 786432
Async XLA Ops:
  0.0 0.7 copy-start

commit v3 on v2

--- a/solution.py
+++ b/solution.py
@@ -60,7 +60,7 @@
 PACK = VALUE_W + 16
 
 
-def mix(n_sp, n_tp, operands, scratch, ready, sent_states, got_states):
+def mix(n_sp, n_tp, operands, scratch, ready, sent_states, loaded, got_states, sent_parts):
     q1, k1, v1, g1, d1, q2, k2, v2, g2, d2, norm1, norm2, out1, out2, res, gain = operands
     cum, qd, kd, added, ends, sent, got, carried, total, mixed, part_send, part_got = scratch[:12]
     fade_own, fade_all, half_send, half_got = scratch[12:16]
@@ -244,6 +244,7 @@
             half_send[u] = carried[:, u].astype(jnp.bfloat16)
             half_copy(u).start()
         got_states()
+        loaded()
         for u in range(count):
             place_copy(u, 0).wait()
             half_copy(u).wait()
@@ -325,6 +326,7 @@
                 value = value + part_got[mask | earlier].astype(jnp.float32)
         part_send[mask] = value.astype(jnp.bfloat16)
         part_copy(mask, bit).start()
+    sent_parts()
     value = project(0)
     for bit in bits:
         part_copy(bit, bit).wait_recv()
@@ -387,7 +389,9 @@
 def mixer_kernel(n_sp, n_tp, *refs):
     operands, (stream_ref, normed_ref), scratch = refs[:16], refs[16:18], refs[18:]
     ready = lambda go: [] if go is None else None
-    stream, normed, pending = mix(n_sp, n_tp, operands, scratch, ready, nothing, nothing)
+    stream, normed, pending = mix(
+        n_sp, n_tp, operands, scratch, ready, nothing, nothing, nothing, nothing
+    )
     stream_ref[...] = stream
     normed_ref[...] = normed
     for one in pending:
@@ -409,22 +413,29 @@
     )(*mix_operands(args, residual, norm_gain))
 
 
-def nearest(place, rank):
-    half, last = GROUPS // 2, GROUPS - 1
-    turned = place // half
-    inner = place + turned * (last - 2 * place)
-    spot = rank + turned * 0
-    if isinstance(rank, int):
-        spot = rank + inner * (1 - 2 * rank) if rank < half else rank + 0 * inner
-    return spot + turned * (last - 2 * spot)
-
-
-def rank_of(place, other):
-    half, last = GROUPS // 2, GROUPS - 1
-    turned = place // half
-    inner = place + turned * (last - 2 * place)
-    spot = other + turned * (last - 2 * other)
-    return spot + inner * (1 - spot // half) * (1 - 2 * spot)
+ORDER = ((0, 1, 2, 3), (1, 3, 2, 0))
+SEND = ((0, 2, 1, 3), (1, 0, 3, 2))
+
+
+def mirror(place):
+    turned, last = place // (GROUPS // 2), GROUPS - 1
+    return turned, place + turned * (last - 2 * place)
+
+
+def place_at(place, rank, table):
+    turned, inner = mirror(place)
+    end, mid = table[0][rank], table[1][rank]
+    spot = end + inner * (mid - end)
+    return spot + turned * (GROUPS - 1 - 2 * spot)
+
+
+def rank_in(place, other, table):
+    turned, inner = mirror(place)
+    spot = other + turned * (GROUPS - 1 - 2 * other)
+    end, mid = (
+        sum(jnp.where(spot == row[rank], rank, 0) for rank in range(GROUPS)) for row in table
+    )
+    return end + inner * (mid - end)
 
 
 KINDS = 5
@@ -432,13 +443,14 @@
 
 
 def layer_kernel(n_sp, n_tp, stride, over, extra, n_scratch, *refs):
-    operands = refs[:16]
+    given = refs[:16]
     ids, group_share, pair_share, w_gate, w_up, w_down, out_ref = refs[16:23]
     scratch = refs[23 : 23 + n_scratch]
+    operands = refs[23 + n_scratch : 39 + n_scratch]
     (
         v_gate, v_up, wd, spread, meta_send, meta_got, wslot, z_send, z_extra, data, hid, hgot,
-        acc, part, pgot, outs, back_got, kept, w_sem, s_sem, r_sem, zs_sem, zr_sem,
-    ) = refs[23 + n_scratch :]
+        acc, part, pgot, outs, back_got, kept, w_sem, o_sem, s_sem, r_sem, zs_sem, zr_sem,
+    ) = refs[39 + n_scratch :]
     bf, f32 = jnp.bfloat16, jnp.float32
     sp, tp = lax.axis_index("sp"), lax.axis_index("tp")
     span = stride + extra
@@ -449,11 +461,14 @@
     place, side = sp // 2, lax.rem(sp, 2)
     core, across, along = (sp, flip_bit(tp, 1)), (sp, flip_bit(tp, 2)), (flip_bit(sp, 1), tp)
     corner = (flip_bit(sp, 1), flip_bit(tp, 2))
-    left, right = slice(0, width // 2), slice(width // 2, width)
-    far = []
+    cut = width // 256 * 128
+    left, right = slice(0, cut), slice(cut, width)
+    far, home = [], []
     for i in range(1, GROUPS):
-        z = nearest(place, i)
-        far.append((i, rank_of(z, place), (z * 2 + side, tp)))
+        z = place_at(place, i, SEND)
+        far.append((i, rank_in(z, place, ORDER), (z * 2 + side, tp)))
+        z = place_at(place, i, ORDER)
+        home.append((i, rank_in(z, place, SEND), (z * 2 + side, tp)))
     numbers = iter(range(COPIES))
     started = []
 
@@ -481,14 +496,21 @@
             ((w_gate, v_gate), (w_up, v_up), (w_down, wd.at[0]))
         )
     ]
-    early = units // 2
+    late = (3, 8, 10, 11, 12, 13, 14, 15)
+    moves = [
+        pltpu.make_async_copy(given[i], operands[i], o_sem.at[i]) for i in range(len(operands))
+    ]
+    quarter = units // 4
     down_y = [
         copy(w_down.at[rows], wd.at[1, rows], along)
-        for rows in (slice(0, early), slice(early, units))
+        for rows in (
+            slice(0, quarter), slice(quarter, 3 * quarter), slice(3 * quarter, units)
+        )
     ]
     down_x = copy(w_down, wd.at[2], across)
-    upper, lower = slice(0, units // 2), slice(units // 2, units)
-    down_yx = copy(wd.at[1, upper], wd.at[3, upper], across)
+    upper, middle = slice(0, quarter), slice(quarter, 2 * quarter)
+    lower = slice(2 * quarter, units)
+    down_yx = [copy(wd.at[1, rows], wd.at[3, rows], across) for rows in (upper, middle)]
     down_xy = copy(wd.at[2, lower], wd.at[3, lower], along)
     metas = [
         z_copy(4, i, rank, meta_send.at[slice(i * span, (i + 1) * span)], meta_got.at[rank], to)
@@ -516,8 +538,8 @@
         counts = contract(member.astype(bf), before.astype(bf), NN)
         nth = jnp.sum(member * counts, axis=0, keepdims=True)
         named = lax.rem(kind, GROUPS)
-        base = (rank_of(place, named) * span).astype(f32)
-        shift = (rank_of(named, place) * over).astype(f32)
+        base = (rank_in(place, named, SEND) * span).astype(f32)
+        shift = (rank_in(named, place, ORDER) * over).astype(f32)
         seat = base + jnp.where(nth < stride, nth, nth + shift)
         seat = jnp.sum(member * seat, axis=0, keepdims=True)
         pair = pair_share[0:1, :] + pair_share[1:2, :]
@@ -546,8 +568,19 @@
     def ready(begin):
         if begin is None:
             return [corner]
+        go(down_x)
+        go(down_y[0])
         for load in loads:
             load.start()
+        for i, move in enumerate(moves):
+            if i not in late:
+                move.wait()
+
+    def sent_states():
+        go(down_y[1])
+        routing()
+        for one in metas:
+            go(one)
         rest = slice(GROUPS * stride + wire, length)
         if wire < extra:
             data[:, rest, :] = jnp.zeros((8, extra - wire, width), bf)
@@ -556,14 +589,15 @@
             for i in range(GROUPS):
                 spare = slice(i * span + stride + wire, (i + 1) * span)
                 back_got[spare, :] = jnp.zeros((extra - wire, width), bf)
-        go(down_x)
-        go(down_y[0])
-        routing()
-        for one in metas:
-            go(one)
-
-    def sent_states():
-        go(down_y[1])
+    def loaded():
+        for i in late:
+            moves[i].wait()
+
+    def sent_parts():
+        down_y[1].wait_recv()
+        go(down_yx[1])
+        down_x.wait_recv()
+        go(down_xy)
 
     def meta_wait(o):
         z_copy(4, 0, o, meta_send.at[block(o)], meta_got.at[o], core).wait_recv()
@@ -578,8 +612,15 @@
             more = more + meta_got[o, stride:].astype(f32)
         wslot[0, GROUPS * stride :] = more.astype(bf)
         go(meta_core)
-
-    stream, normed, pending = mix(n_sp, n_tp, operands, scratch, ready, sent_states, got_states)
+        down_y[0].wait_recv()
+        go(down_yx[0])
+        go(down_y[2])
+
+    for i in sorted(range(len(moves)), key=lambda i: i in late):
+        moves[i].start()
+    stream, normed, pending = mix(
+        n_sp, n_tp, operands, scratch, ready, sent_states, loaded, got_states, sent_parts
+    )
     kept[...] = stream
 
     for i, rank, to in far:
@@ -715,7 +756,7 @@
         if o == 0:
             back_got[0:stride] = outs[rows, :]
         else:
-            i, rank, to = far[o - 1]
+            i, rank, to = home[o - 1]
             go(
                 z_copy(
                     2, i, rank,
@@ -727,7 +768,7 @@
         if o == GROUPS - 1:
             rows = slice(GROUPS * stride, GROUPS * stride + wire)
             back_got[stride : stride + wire] = outs[rows, :]
-            for i, rank, to in far:
+            for i, rank, to in home:
                 go(
                     z_copy(
                         3, i, rank,
@@ -739,36 +780,31 @@
 
     stage(0)
     forward(0)
-    stage(1)
     for load in loads:
         load.wait()
     finish(0)
     compute(0)
+    stage(1)
     forward(1)
-    down_y[0].wait_recv()
-    down_y[1].wait_recv()
-    go(down_yx)
-    down_x.wait_recv()
-    go(down_xy)
     stage(2)
     finish(1)
     compute(1)
     forward(2)
     stage(3)
     meta_core.wait_recv()
-    down_yx.wait_recv()
-    down_xy.wait_recv()
+    for one in (down_y[2], *down_yx, down_xy):
+        one.wait_recv()
     down(0)
+    down(1)
     finish(2)
     compute(2)
-    down(1)
+    give(1)
     forward(3)
-    give(0)
-    give(1)
     down(2)
     finish(3)
     compute(3)
     give(2)
+    give(0)
     down(3)
     give(3)
     for i in range(1, GROUPS):
@@ -792,12 +828,14 @@
     hbm = pl.BlockSpec(memory_space=pl.ANY)
     sem = pltpu.SemaphoreType.DMA
     mine = mix_scratch(n_sp, n_tp, args, residual)
+    given = mix_operands(args, residual, norm_gain)
     return pl.pallas_call(
         functools.partial(layer_kernel, n_sp, n_tp, stride, over, extra, len(mine)),
         out_shape=jax.ShapeDtypeStruct((rows, width), bf),
-        in_specs=[vmem] * 19 + [hbm] * 3,
+        in_specs=[hbm] * 16 + [vmem] * 3 + [hbm] * 3,
         out_specs=vmem,
         scratch_shapes=mine
+        + [pltpu.VMEM(one.shape, one.dtype) for one in given]
         + [
             pltpu.VMEM(w_gate.shape, bf),
             pltpu.VMEM(w_up.shape, bf),
@@ -818,6 +856,7 @@
             pltpu.VMEM((GROUPS * span, width), bf),
             pltpu.VMEM((rows, width), bf),
             sem((3,)),
+            sem((16,)),
             sem((COPIES,)),
             sem((COPIES,)),
             sem((KINDS * GROUPS,)),
@@ -826,7 +865,7 @@
         compiler_params=pltpu.CompilerParams(
             collective_id=1, has_side_effects=True, vmem_limit_bytes=63 * 2**20
         ),
-    )(*mix_operands(args, residual, norm_gain), *routing, w_gate, w_up, w_down)
+    )(*given, *routing, w_gate, w_up, w_down)
 
 
 def slot_table(routes, capacity, experts):

time: 131 us -> 119 us (0.908)
  Pallas kernels: 128 us -> 116 us
    pallas_call x1, Pallas kernels: 128 us -> 116 us  [whole_layer(): pl.pallas_call(functools.partial(layer_kernel, n_sp, n_tp, stride, over,...]
where the time goes in v3:
time: 119 us
  Pallas kernels  116 us (97%)
  local copies, waits for them, and re-layouts  3.01 us (3%)
    pallas_call x1, Pallas kernels, whole_layer(): pl.pallas_call(functools.partial(layer_kernel, n_sp, n_tp, stride, over,...  116 us
    unnamed x3, local copies, waits for them, and re-layouts  2.45 us

profile of v3, /device:TPU:0, one launch (start us, length us, event | category | flops | bytes accessed | tf_op | source)
XLA Modules:
  0.0 119.2 jit_solution(10398108065534312098)
XLA Ops:
  0.0 0.0 copy-start
  0.0 0.7 copy-done
  0.7 0.6 broadcast_in_dim.15.refs_17_
  1.2 116.2 %shard_map.208 = bf16[96,2048]{1,0:T(8,128)(2,1)} custom-call(bf16[384,128]{1,0:T(8,128)(2,1)} %refs_0_.1, bf16[384,128]{1,0:T(8,128)(2,1)} %refs_1_.1, bf16[384,256]{1,0:T(8,128)(2,1)} %refs_2_.1, bf16[384,256]{1,0:T(8,128)(2,1)} %refs_3_.1, bf16[2,384,128]{2,1,0:T(8,128)(2,1)} %refs_4_.1, bf16[384,256]{1,0:T(8,128)(2,1)} %refs_5_.1, ...), custom_call_target="tpu_custom_call" | custom-call | tf_op jit(solution)/shard_map/pallas_call | solution.py:832
  117.5 1.8 %copy.24 = bf16[96,2048]{1,0:T(8,128)(2,1)} copy(bf16[96,2048]{1,0:T(8,128)(2,1)} %shard_map.208) | data formatting | bytes 786432
Async XLA Ops:
  0.0 0.7 copy-start

commit v4 on v3

--- a/solution.py
+++ b/solution.py
@@ -700,13 +700,13 @@
         flow["b_d"].wait_recv()
         go(flow["c_d"])
 
-    def compute(o):
+    def compute(o, part_at):
         flow, ch = flows[o], chunk(o)
-        for name in ("c_0", "c_y", "c_x", "c_d"):
+        for name in (("c_0", "c_y"), ("c_x", "c_d"))[part_at]:
             flow[name].wait_recv()
         n = ch.stop - ch.start
 
-        @pl.loop(0, 2)
+        @pl.loop(part_at, part_at + 1)
         def _(m):
             some = pl.ds(m * 4, 4)
             x = data[some, ch, :].reshape(4 * n, width)
@@ -715,7 +715,7 @@
             hidden = (gate / (1.0 + jnp.exp(-gate)) * up).astype(bf)
             hid[some, ch, :] = hidden.reshape(4, n, units)
 
-        for name in ("h_y", "h_x", "h_d"):
+        for name in (("h_y",), ("h_d", "h_x"))[part_at]:
             go(flow[name])
 
     lane = lax.broadcasted_iota(jnp.int32, (1, 128), 1)
@@ -782,13 +782,15 @@
     forward(0)
     for load in loads:
         load.wait()
+    compute(0, 0)
     finish(0)
-    compute(0)
+    compute(0, 1)
     stage(1)
     forward(1)
     stage(2)
+    compute(1, 0)
     finish(1)
-    compute(1)
+    compute(1, 1)
     forward(2)
     stage(3)
     meta_core.wait_recv()
@@ -796,13 +798,15 @@
         one.wait_recv()
     down(0)
     down(1)
+    compute(2, 0)
     finish(2)
-    compute(2)
+    compute(2, 1)
     give(1)
     forward(3)
     down(2)
+    compute(3, 0)
     finish(3)
-    compute(3)
+    compute(3, 1)
     give(2)
     give(0)
     down(3)

time: 119 us -> 118 us (level)
  Pallas kernels: 116 us -> 114 us
    pallas_call x1, Pallas kernels: 116 us -> 114 us  [whole_layer(): pl.pallas_call(functools.partial(layer_kernel, n_sp, n_tp, stride, over,...]
where the time goes in v4:
time: 118 us; the launch traced here: 117 us
  Pallas kernels  114 us (97%)
  local copies, waits for them, and re-layouts  3.01 us (3%)
    pallas_call x1, Pallas kernels, whole_layer(): pl.pallas_call(functools.partial(layer_kernel, n_sp, n_tp, stride, over,...  114 us
    unnamed x3, local copies, waits for them, and re-layouts  2.45 us

profile of v4, /device:TPU:0, one launch (start us, length us, event | category | flops | bytes accessed | tf_op | source)
XLA Modules:
  0.0 117.3 jit_solution(6160195626655929816)
XLA Ops:
  0.0 0.0 copy-start
  0.0 0.7 copy-done
  0.7 0.6 broadcast_in_dim.15.refs_17_
  1.2 114.3 %shard_map.208 = bf16[96,2048]{1,0:T(8,128)(2,1)} custom-call(bf16[384,128]{1,0:T(8,128)(2,1)} %refs_0_.1, bf16[384,128]{1,0:T(8,128)(2,1)} %refs_1_.1, bf16[384,256]{1,0:T(8,128)(2,1)} %refs_2_.1, bf16[384,256]{1,0:T(8,128)(2,1)} %refs_3_.1, bf16[2,384,128]{2,1,0:T(8,128)(2,1)} %refs_4_.1, bf16[384,256]{1,0:T(8,128)(2,1)} %refs_5_.1, ...), custom_call_target="tpu_custom_call" | custom-call | tf_op jit(solution)/shard_map/pallas_call | solution.py:836
  115.5 1.8 %copy.24 = bf16[96,2048]{1,0:T(8,128)(2,1)} copy(bf16[96,2048]{1,0:T(8,128)(2,1)} %shard_map.208) | data formatting | bytes 786432
Async XLA Ops:
  0.0 0.7 copy-start
